TPU v7x, 512 devices: a whole 4x8x8 slice. The times are simulated.
512 devices in a mesh: tp: 64 (over z, y), dp: 8 (over x, core).
Axes of the slice: x: 4, y: 8, z: 8, core: 2. Of those that a mesh axis runs over, the one named last changes fastest.
Arguments:
- tokens: bfloat16 [256, 4096], P(None, 'dp'), may hold values from -6 to 6
- lengths: int32 [256], P('dp'), may hold values from 1 to 4096, 262144 in all
- norm_gain: float32 [2, 4096], P(None, 'dp'), may hold values from 0.1 to 1.9
- w_in: bfloat16 [2, 4096, 2048], P(None, 'dp', 'tp'), may hold values from -0.09375 to 0.09375
- log_step: float32 [2, 128], P(None, 'tp'), may hold values from -4.6 to -0.7
- eig_re: float32 [2, 128, 64], P(None, 'tp'), may hold values from -2 to -0.05
- eig_im: float32 [2, 128, 64], P(None, 'tp'), may hold values from 0 to 8
- in_mat: float32 [2, 2, 128, 64, 16], P(None, None, 'tp'), may hold values from -2.5 to 2.5
- output_matrices: float32 [2, 2, 128, 16, 64], P(None, None, 'tp'), may hold values from -1.25 to 1.25
- skip: float32 [2, 2048], P(None, 'tp'), may hold values from -4 to 4
- w_glu: bfloat16 [2, 2048, 4096], P(None, 'tp', 'dp'), may hold values from -0.75 to 0.75
- w_gate: bfloat16 [2, 2048, 4096], P(None, 'tp', 'dp'), may hold values from -0.125 to 0.125
- state: float32 [2, 2, 256, 8192], P(None, None, 'dp', 'tp'), may hold values from -6 to 6
Outputs:
- mixed: bfloat16 [256, 4096], P(None, 'dp')
- new_state: float32 [2, 2, 256, 8192], P(None, None, 'dp', 'tp')
Inputs may be any that keep to these rules, and one draw needn't show every extreme that they name: `lengths`: each sequence's number of past positions; the largest is exactly 4096 and all add up to 262144.
All inputs are finite; a program needn't handle non-finite values.
Results may differ from a plain program's by a relative error of at most 0.0095.
Values may be sent and summed in bfloat16 or wider, within the bound.
A program may use at most 64 MiB of HBM per device.

v0:
```python
import math

import jax
import jax.numpy as jnp
from jax import lax
from jax.sharding import PartitionSpec as P

D = 4096
GROUP = 16
STATES = 64
LAYERS = 2
LEN_MAX = 4096
BLOCK_LEN = 256


NORM_EPS = 1e-06
FULL_PRECISION = lax.Precision.HIGHEST


def split_up(array, dim, length):
    before, after = (array.shape[:dim], array.shape[dim + 1 :])
    return jnp.moveaxis(array.reshape(*before, length, -1, *after), dim, 0)


def sent_and_summed(array, axis, dim):
    pieces = split_up(array, dim, lax.axis_size(axis))
    arrived = lax.all_to_all(pieces, axis, split_axis=0, concat_axis=0, tiled=True)
    return arrived.sum(axis=0)


def sent_together(arrays, axis, dim, along):
    widths = [math.prod(a.shape[along:]) for a in arrays]
    both = jnp.concatenate(
        [a.reshape(*a.shape[:along], w) for a, w in zip(arrays, widths)], axis=along
    )
    out = sent_and_summed(both, axis, dim)
    pieces = jnp.split(out, [sum(widths[:k]) for k in range(1, len(widths))], axis=along)
    return tuple((b.reshape(*out.shape[:along], *a.shape[along:]) for a, b in zip(arrays, pieces)))


def joined_along(pieces, dim):
    pieces = jnp.moveaxis(pieces, 0, dim)
    lengths = pieces.shape
    return pieces.reshape(*lengths[:dim], lengths[dim] * lengths[dim + 1], *lengths[dim + 2 :])


def sent_to_all(array, axis):
    length = lax.axis_size(axis)
    return lax.all_to_all(
        jnp.broadcast_to(array[None], (length, *array.shape)), axis, 0, 0, tiled=True
    )


def gathered_copies(array, axis, dim):
    return joined_along(sent_to_all(array, axis), dim)


def position_factor(lengths):
    blocks = (lengths // BLOCK_LEN).astype(jnp.float32)
    return 2.0 / (1.0 + blocks * (4.0 * BLOCK_LEN / LEN_MAX))


def recurrent_step(
    driven_state, state_pair, factor, log_step, eig_re, eig_im, in_mat, output_matrices, skip
):
    step_size = jnp.exp(log_step)[None, :, None] * factor[:, None, None]
    magnitude = jnp.exp(eig_re[None] * step_size)
    turned = eig_im[None] * step_size
    decay_re = magnitude * jnp.cos(turned)
    decay_im = magnitude * jnp.sin(turned)
    modulus = eig_re * eig_re + eig_im * eig_im
    weight_re = ((decay_re - 1.0) * eig_re + decay_im * eig_im) / modulus
    weight_im = (decay_im * eig_re - (decay_re - 1.0) * eig_im) / modulus
    drive_re = jnp.einsum("bgc,gpc->bgp", driven_state, in_mat[0], precision=FULL_PRECISION)
    drive_im = jnp.einsum("bgc,gpc->bgp", driven_state, in_mat[1], precision=FULL_PRECISION)
    state_real = (
        decay_re * state_pair[0]
        - decay_im * state_pair[1]
        + weight_re * drive_re
        - weight_im * drive_im
    )
    state_imaginary = (
        decay_re * state_pair[1]
        + decay_im * state_pair[0]
        + weight_re * drive_im
        + weight_im * drive_re
    )
    readout_value = (
        jnp.einsum("szv,zuv->szu", state_real, output_matrices[0], precision=FULL_PRECISION)
        - jnp.einsum("szv,zuv->szu", state_imaginary, output_matrices[1], precision=FULL_PRECISION)
        + skip * driven_state
    )
    return (jax.nn.gelu(readout_value), state_real, state_imaginary)


def body(
    tokens,
    lengths,
    norm_gain,
    w_in,
    log_step,
    eig_re,
    eig_im,
    in_mat,
    output_matrices,
    skip,
    w_glu,
    w_gate,
    state,
):
    factor = position_factor(lengths)
    current = tokens.astype(jnp.float32)
    rounded = tokens
    new_states = []
    for layer_index in range(LAYERS):
        squares = jnp.sum(current * current, axis=1)
        scaled = (current * norm_gain[layer_index]).astype(jnp.bfloat16)
        partial_value = jnp.dot(scaled, w_in[layer_index], preferred_element_type=jnp.float32)
        summed, total_squares = sent_together((partial_value, squares), "dp", 0, 1)
        driven_state = (summed * lax.rsqrt(total_squares / D + NORM_EPS)[:, None]).astype(
            jnp.bfloat16
        )
        own_seqs = driven_state.shape[0]
        group_count = log_step.shape[1]
        driven_state = driven_state.astype(jnp.float32).reshape(own_seqs, group_count, GROUP)
        state_pair = state[layer_index].reshape(2, own_seqs, group_count, STATES)
        readout_value, state_real, state_imaginary = recurrent_step(
            driven_state,
            state_pair,
            factor,
            log_step[layer_index],
            eig_re[layer_index],
            eig_im[layer_index],
            in_mat[layer_index],
            output_matrices[layer_index],
            skip[layer_index].reshape(group_count, GROUP),
        )
        readout_value = readout_value.reshape(own_seqs, group_count * GROUP).astype(jnp.bfloat16)
        new_states.append(
            jnp.stack([state_real, state_imaginary]).reshape(2, own_seqs, group_count * STATES)
        )
        glu_weight = w_glu[layer_index]
        gate_matrix = w_gate[layer_index]
        piece = gathered_copies(readout_value, "dp", 0)
        combined_terms = jnp.stack(
            [
                jnp.dot(piece, glu_weight, preferred_element_type=jnp.float32),
                jnp.dot(piece, gate_matrix, preferred_element_type=jnp.float32),
            ]
        )
        share = sent_and_summed(combined_terms, "tp", 2)
        width = share.shape[2]
        own_cols = lax.dynamic_slice_in_dim(current, lax.axis_index("tp") * width, width, 1)
        piece_out = (own_cols + share[0] * jax.nn.sigmoid(share[1])).astype(jnp.bfloat16)
        rounded = gathered_copies(piece_out, "tp", 1)
        current = rounded.astype(jnp.float32)
    return (rounded, jnp.stack(new_states))


def solution(mesh):
    placed = (
        P(None, "dp"),
        P("dp"),
        P(None, "dp"),
        P(None, "dp", "tp"),
        P(None, "tp"),
        P(None, "tp", None),
        P(None, "tp", None),
        P(None, None, "tp", None, None),
        P(None, None, "tp", None, None),
        P(None, "tp"),
        P(None, "tp", "dp"),
        P(None, "tp", "dp"),
        P(None, None, "dp", "tp"),
    )
    return jax.shard_map(
        body,
        mesh=mesh,
        in_specs=placed,
        out_specs=(P(None, "dp"), P(None, None, "dp", "tp")),
        check_vma=False,
    )
```

profile of v0, /device:TPU:1, one launch (start us, length us, event | category | flops | bytes accessed | tf_op | source)
XLA Modules:
  0.0 176.6 jit_solution(547062946090717240)
XLA Ops:
  0.6 1.1 copy.102
  3.2 0.8 reshape.256
  4.0 10.2 %all-to-all-start = ((f32[8,1,1056]{2,1,0:T(1,128)}), f32[8,1,1056]{2,1,0:T(1,128)S(1)}, u32[]{:S(2)}, u32[]{:S(2)}) async-start(f32[8,1,1056]{2,1,0:T(1,128)} %reshape.256), calls=%async_computation | async-start | bytes 73728 | tf_op jit(solution)/shard_map/all_to_all | solution.py:27
  14.2 0.7 copy-done.9
  14.9 0.6 copy-done.11
  15.6 0.6 copy-done.7
  17.2 1.7 all-to-all-done
  19.5 0.7 reduce.18
  22.7 0.7 reshape.258
  23.4 4.0 %all-to-all-start.1 = ((bf16[8,2,512]{2,1,0:T(2,128)(2,1)}), bf16[8,2,512]{2,1,0:T(2,128)(2,1)S(1)}, u32[]{:S(2)}, u32[]{:S(2)}) async-start(bf16[8,2,512]{2,1,0:T(2,128)(2,1)} %reshape.258), calls=%async_computation.1 | async-start | bytes 32768 | tf_op jit(solution)/shard_map/all_to_all | solution.py:49
  27.6 4.4 %all-to-all-done.1 = bf16[8,2,512]{2,1,0:T(2,128)(2,1)S(1)} async-done(((bf16[8,2,512]{2,1,0:T(2,128)(2,1)}), bf16[8,2,512]{2,1,0:T(2,128)(2,1)S(1)}, u32[]{:S(2)}, u32[]{:S(2)}) %all-to-all-start.1) | async-done | bytes 16416 | tf_op jit(solution)/shard_map/all_to_all | solution.py:49
  32.8 1.6 copy.115
  34.4 12.0 %all-to-all-start.2 = ((f32[64,2,256,8]{2,3,1,0:T(8,128)}), f32[64,2,256,8]{2,3,1,0:T(8,128)S(1)}, u32[]{:S(2)}, u32[]{:S(2)}) async-start(f32[64,2,256,8]{2,3,1,0:T(8,128)} %copy.115), calls=%async_computation.2 | async-start | bytes 2097152 | tf_op jit(solution)/shard_map/all_to_all | solution.py:27
  46.5 27.4 %all-to-all-done.2 = f32[64,2,256,8]{2,3,1,0:T(8,128)S(1)} async-done(((f32[64,2,256,8]{2,3,1,0:T(8,128)}), f32[64,2,256,8]{2,3,1,0:T(8,128)S(1)}, u32[]{:S(2)}, u32[]{:S(2)}) %all-to-all-start.2) | async-done | bytes 1048608 | tf_op jit(solution)/shard_map/all_to_all | solution.py:27
  74.0 0.7 broadcast_in_dim.9
  74.7 7.8 %all-to-all-start.3 = ((bf16[64,256,8]{1,2,0:T(8,128)(2,1)}), bf16[64,256,8]{1,2,0:T(8,128)(2,1)S(1)}, u32[]{:S(2)}, u32[]{:S(2)}) async-start(bf16[64,256,8]{1,2,0:T(8,128)(2,1)} %broadcast_in_dim.9), calls=%async_computation.3 | async-start | bytes 524288 | tf_op jit(solution)/shard_map/all_to_all | solution.py:49
  82.6 12.5 %all-to-all-done.3 = bf16[64,256,8]{1,2,0:T(8,128)(2,1)S(1)} async-done(((bf16[64,256,8]{1,2,0:T(8,128)(2,1)}), bf16[64,256,8]{1,2,0:T(8,128)(2,1)S(1)}, u32[]{:S(2)}, u32[]{:S(2)}) %all-to-all-start.3) | async-done | bytes 262176 | tf_op jit(solution)/shard_map/all_to_all | solution.py:49
  96.4 0.8 reshape.260
  97.2 6.7 %all-to-all-start.4 = ((f32[8,1,1056]{2,1,0:T(1,128)}), f32[8,1,1056]{2,1,0:T(1,128)S(1)}, u32[]{:S(2)}, u32[]{:S(2)}) async-start(f32[8,1,1056]{2,1,0:T(1,128)} %reshape.260), calls=%async_computation.4 | async-start | bytes 73728 | tf_op jit(solution)/shard_map/all_to_all | solution.py:27
  104.1 4.5 %all-to-all-done.4 = f32[8,1,1056]{2,1,0:T(1,128)S(1)} async-done(((f32[8,1,1056]{2,1,0:T(1,128)}), f32[8,1,1056]{2,1,0:T(1,128)S(1)}, u32[]{:S(2)}, u32[]{:S(2)}) %all-to-all-start.4) | async-done | bytes 33824 | tf_op jit(solution)/shard_map/all_to_all | solution.py:27
  108.6 0.7 reduce.19
  110.8 0.7 reshape.262
  111.5 4.0 %all-to-all-start.5 = ((bf16[8,2,512]{2,1,0:T(2,128)(2,1)}), bf16[8,2,512]{2,1,0:T(2,128)(2,1)S(1)}, u32[]{:S(2)}, u32[]{:S(2)}) async-start(bf16[8,2,512]{2,1,0:T(2,128)(2,1)} %reshape.262), calls=%async_computation.5 | async-start | bytes 32768 | tf_op jit(solution)/shard_map/all_to_all | solution.py:49
  115.7 4.4 %all-to-all-done.5 = bf16[8,2,512]{2,1,0:T(2,128)(2,1)S(1)} async-done(((bf16[8,2,512]{2,1,0:T(2,128)(2,1)}), bf16[8,2,512]{2,1,0:T(2,128)(2,1)S(1)}, u32[]{:S(2)}, u32[]{:S(2)}) %all-to-all-start.5) | async-done | bytes 16416 | tf_op jit(solution)/shard_map/all_to_all | solution.py:49
  120.9 1.6 copy.129
  122.5 4.7 %all-to-all-start.6 = ((f32[64,2,256,8]{2,3,1,0:T(8,128)}), f32[64,2,256,8]{2,3,1,0:T(8,128)S(1)}, u32[]{:S(2)}, u32[]{:S(2)}) async-start(f32[64,2,256,8]{2,3,1,0:T(8,128)} %copy.129), calls=%async_computation.6 | async-start | bytes 2097152 | tf_op jit(solution)/shard_map/all_to_all | solution.py:27
  127.2 27.5 %all-to-all-done.6 = f32[64,2,256,8]{2,3,1,0:T(8,128)S(1)} async-done(((f32[64,2,256,8]{2,3,1,0:T(8,128)}), f32[64,2,256,8]{2,3,1,0:T(8,128)S(1)}, u32[]{:S(2)}, u32[]{:S(2)}) %all-to-all-start.6) | async-done | bytes 1048608 | tf_op jit(solution)/shard_map/all_to_all | solution.py:27
  154.8 0.7 broadcast_in_dim.11
  155.6 7.7 %all-to-all-start.7 = ((bf16[64,256,8]{1,2,0:T(8,128)(2,1)}), bf16[64,256,8]{1,2,0:T(8,128)(2,1)S(1)}, u32[]{:S(2)}, u32[]{:S(2)}) async-start(bf16[64,256,8]{1,2,0:T(8,128)(2,1)} %broadcast_in_dim.11), calls=%async_computation.7 | async-start | bytes 524288 | tf_op jit(solution)/shard_map/all_to_all | solution.py:49
  163.7 0.6 maximum_maximum_fusion
  164.4 11.4 %all-to-all-done.7 = bf16[64,256,8]{1,2,0:T(8,128)(2,1)S(1)} async-done(((bf16[64,256,8]{1,2,0:T(8,128)(2,1)}), bf16[64,256,8]{1,2,0:T(8,128)(2,1)S(1)}, u32[]{:S(2)}, u32[]{:S(2)}) %all-to-all-start.7) | async-done | bytes 262176 | tf_op jit(solution)/shard_map/all_to_all | solution.py:49
  175.8 0.8 copy.135
  (98 shorter events, 11.1 us)
Async XLA Ops:
  0.6 1.1 copy-start.6
  2.1 0.8 copy-start.5
  4.0 10.2 %copy-start = (f32[2,2,32,128]{3,2,1,0:T(8,128)S(1)}, f32[2,2,32,128]{3,2,1,0:T(8,128)}, u32[]{:S(2)}) copy-start(f32[2,2,32,128]{3,2,1,0:T(8,128)} %param.25) | copy-start | bytes 196612
  4.0 15.0 %all-to-all-start = ((f32[8,1,1056]{2,1,0:T(1,128)}), f32[8,1,1056]{2,1,0:T(1,128)S(1)}, u32[]{:S(2)}, u32[]{:S(2)}) async-start(f32[8,1,1056]{2,1,0:T(1,128)} %reshape.256), calls=%async_computation | async-start | bytes 73728 | tf_op jit(solution)/shard_map/all_to_all | solution.py:27
  14.2 0.7 copy-start.9
  14.2 1.4 copy-start.1
  14.9 0.7 copy-start.11
  15.6 0.7 copy-start.7
  15.6 0.7 copy-start.8
  16.3 0.7 copy-start.10
  20.4 0.8 copy-start.4
  21.4 0.8 copy-start.3
  22.7 4.7 %copy-start.2 = (bf16[2,32,512]{2,1,0:T(8,128)(2,1)S(1)}, bf16[2,32,512]{2,1,0:T(8,128)(2,1)}, u32[]{:S(2)}) copy-start(bf16[2,32,512]{2,1,0:T(8,128)(2,1)} %param.23) | copy-start | bytes 196612
  23.4 8.6 %all-to-all-start.1 = ((bf16[8,2,512]{2,1,0:T(2,128)(2,1)}), bf16[8,2,512]{2,1,0:T(2,128)(2,1)S(1)}, u32[]{:S(2)}, u32[]{:S(2)}) async-start(bf16[8,2,512]{2,1,0:T(2,128)(2,1)} %reshape.258), calls=%async_computation.1 | async-start | bytes 32768 | tf_op jit(solution)/shard_map/all_to_all | solution.py:49
  34.4 39.5 %all-to-all-start.2 = ((f32[64,2,256,8]{2,3,1,0:T(8,128)}), f32[64,2,256,8]{2,3,1,0:T(8,128)S(1)}, u32[]{:S(2)}, u32[]{:S(2)}) async-start(f32[64,2,256,8]{2,3,1,0:T(8,128)} %copy.115), calls=%async_computation.2 | async-start | bytes 2097152 | tf_op jit(solution)/shard_map/all_to_all | solution.py:27
  74.7 20.3 %all-to-all-start.3 = ((bf16[64,256,8]{1,2,0:T(8,128)(2,1)}), bf16[64,256,8]{1,2,0:T(8,128)(2,1)S(1)}, u32[]{:S(2)}, u32[]{:S(2)}) async-start(bf16[64,256,8]{1,2,0:T(8,128)(2,1)} %broadcast_in_dim.9), calls=%async_computation.3 | async-start | bytes 524288 | tf_op jit(solution)/shard_map/all_to_all | solution.py:49
  97.2 11.4 %all-to-all-start.4 = ((f32[8,1,1056]{2,1,0:T(1,128)}), f32[8,1,1056]{2,1,0:T(1,128)S(1)}, u32[]{:S(2)}, u32[]{:S(2)}) async-start(f32[8,1,1056]{2,1,0:T(1,128)} %reshape.260), calls=%async_computation.4 | async-start | bytes 73728 | tf_op jit(solution)/shard_map/all_to_all | solution.py:27
  111.5 8.6 %all-to-all-start.5 = ((bf16[8,2,512]{2,1,0:T(2,128)(2,1)}), bf16[8,2,512]{2,1,0:T(2,128)(2,1)S(1)}, u32[]{:S(2)}, u32[]{:S(2)}) async-start(bf16[8,2,512]{2,1,0:T(2,128)(2,1)} %reshape.262), calls=%async_computation.5 | async-start | bytes 32768 | tf_op jit(solution)/shard_map/all_to_all | solution.py:49
  122.5 32.2 %all-to-all-start.6 = ((f32[64,2,256,8]{2,3,1,0:T(8,128)}), f32[64,2,256,8]{2,3,1,0:T(8,128)S(1)}, u32[]{:S(2)}, u32[]{:S(2)}) async-start(f32[64,2,256,8]{2,3,1,0:T(8,128)} %copy.129), calls=%async_computation.6 | async-start | bytes 2097152 | tf_op jit(solution)/shard_map/all_to_all | solution.py:27
  155.6 20.2 %all-to-all-start.7 = ((bf16[64,256,8]{1,2,0:T(8,128)(2,1)}), bf16[64,256,8]{1,2,0:T(8,128)(2,1)S(1)}, u32[]{:S(2)}, u32[]{:S(2)}) async-start(bf16[64,256,8]{1,2,0:T(8,128)(2,1)} %broadcast_in_dim.11), calls=%async_computation.7 | async-start | bytes 524288 | tf_op jit(solution)/shard_map/all_to_all | solution.py:49
where the time goes:
time: 179 us; the launch traced here: 177 us
  waiting for transfers between devices  93.9 us (52%)
  starting transfers between devices  57 us (32%)
  local copies, waits for them, and re-layouts  17.9 us (10%)
  other arithmetic  3.67 us (2%)
  matrix products  3.06 us (2%)
    all_to_all x4, waiting for transfers between devices, sent_and_summed(): lax.all_to_all(pieces, axis, split_axis=0, concat_axis=0, tiled=True)  61.2 us
    all_to_all x4, starting transfers between devices, sent_and_summed(): lax.all_to_all(pieces, axis, split_axis=0, concat_axis=0, tiled=True)  33.5 us
    all_to_all x4, waiting for transfers between devices, sent_to_all(): lax.all_to_all(jnp.broadcast_to(array[None], (length, *array.shape)), axi...  32.7 us
    all_to_all x4, starting transfers between devices, sent_to_all(): lax.all_to_all(jnp.broadcast_to(array[None], (length, *array.shape)), axi...  23.4 us
    unnamed x36, local copies, waits for them, and re-layouts  9.72 us
  transfers between devices with their start and end apart: 8, of which 8 were waited for; matrix products, arithmetic and copies ran while one was open for 1% of the time, Pallas kernels for 0%

commit v1 on v0

v1 whole, which is shorter than its diff:
```python
import jax
import jax.numpy as jnp
from jax import lax
from jax.experimental import pallas as pl
from jax.experimental.pallas import tpu as pltpu
from jax.sharding import PartitionSpec as P

D = 4096
LEN_MAX = 4096
BLOCK_LEN = 256
NORM_EPS = 1e-06
MESH = pl.DeviceIdType.MESH
F32 = jnp.float32
BF16 = jnp.bfloat16

(PH1, ST1A, RES0, PH2, ST1B, ST1W, PH3, PH4, RES1, PH5, PH6, PH7, PH8, PH9A, PH9B, GAIN) = range(16)
NEAR = 16
PAIR = NEAR + 9
COUNT = PAIR + 12


def roll(x, amount):
    amount = amount % 128
    return x if amount == 0 else pltpu.roll(x, amount, 1)


def groups4(rows):
    return lax.broadcasted_iota(jnp.int32, (rows, 128), 1) // 32


def low_half(rows):
    return lax.broadcasted_iota(jnp.int32, (rows, 128), 1) < 64


def pick4(parts, group):
    out = parts[3]
    for i in (2, 1, 0):
        out = jnp.where(group == i, parts[i], out)
    return out


def split2(x):
    hi = x.astype(BF16)
    lo = (x - hi.astype(F32)).astype(BF16)
    return hi, lo


def kernel(
    tok_h, len_h, gain_h, win_h, ls_h, er_h, ei_h, im_h, om_h, skip_h, glu_h, gate_h, st_h,
    mixed_ref, ns_ref,
    tok, lens, gain, win, ls, er, ei, im, om, skip, glu, gate, st,
    s1, r1, ws, w, wis, pk, wi, gb, rz, rz1, s2, r2, s3, r3, r4, m0, s5, r5, s7, r7, oa, ob,
    lsem, ss, rs,
):
    tp = lax.axis_index("tp")
    d = lax.axis_index("dp")
    z = tp // 8
    y = lax.rem(tp, 8)
    x = d // 2
    core = lax.rem(d, 2)

    def at_y(k):
        return {"tp": z * 8 + lax.rem(y + k, 8), "dp": d}

    def at_z(k):
        return {"tp": lax.rem(z + k, 8) * 8 + y, "dp": d}

    def at_d(k):
        return {"tp": tp, "dp": lax.rem(d + k, 8)}

    def send(src, dst, sem, dev, rsem=None):
        pltpu.make_async_remote_copy(
            src_ref=src,
            dst_ref=dst,
            send_sem=ss.at[sem],
            recv_sem=rs.at[sem if rsem is None else rsem],
            device_id=dev,
            device_id_type=MESH,
        ).start()

    def wait_recv(ref, sem):
        pltpu.make_async_copy(ref, ref, rs.at[sem]).wait()

    def wait_sent(ref, sem):
        pltpu.make_async_copy(ref, ref, ss.at[sem]).wait()

    hbm = (tok_h, win_h, gain_h, glu_h, gate_h, len_h, ls_h, er_h, ei_h, im_h, om_h, skip_h, st_h)
    vmem = (tok, win, gain, glu, gate, lens, ls, er, ei, im, om, skip, st)
    loads = [pltpu.make_async_copy(a, b, lsem.at[i]) for i, (a, b) in enumerate(zip(hbm, vmem))]
    for copy in loads:
        copy.start()

    barrier = pltpu.get_barrier_semaphore()
    for k in range(1, 8):
        for dev in (at_d(k), at_y(k), at_z(k)):
            pl.semaphore_signal(barrier, inc=1, device_id=dev, device_id_type=MESH)
    for k in range(8):
        @pl.when(jnp.logical_not(jnp.logical_and(z == k, d == z)))
        def _(k=k):
            pl.semaphore_signal(
                barrier, inc=1, device_id={"tp": k * 8 + y, "dp": z}, device_id_type=MESH
            )

    group8 = groups4(8)
    low16 = low_half(16)
    low32 = low_half(32)

    for i in range(3):
        loads[i].wait()
    for dd in range(8):
        t = tok[32 * dd : 32 * dd + 32, :].astype(F32)
        scaled = (t * gain[0:1, :]).astype(BF16)
        part = jnp.dot(scaled, win[0], preferred_element_type=F32)
        sq = jnp.sum(t * t, axis=1, keepdims=True)
        s1[dd, 0:8, :] = jnp.concatenate([part[8 * i : 8 * i + 8, :] for i in range(4)], axis=1)
        s1[dd, 8:16, :] = pick4(
            [jnp.broadcast_to(sq[8 * i : 8 * i + 8, :], (8, 128)) for i in range(4)], group8
        )
    r1[pl.ds(d, 1)] = s1[pl.ds(d, 1)]

    loads[3].wait()
    loads[4].wait()

    def pack_projection(layer):
        for q in range(4):
            g = glu[layer, :, 128 * q : 128 * q + 128].astype(F32)
            t = gate[layer, :, 128 * q : 128 * q + 128].astype(F32)
            ws[layer, 2 * q] = jnp.where(low32, g, roll(t, 64)).astype(BF16)
            ws[layer, 2 * q + 1] = jnp.where(low32, roll(g, 64), t).astype(BF16)
        w[layer, pl.ds(d, 1), pl.ds(y, 1)] = ws[layer, pl.ds(y, 1)][None]

    pack_projection(0)

    half = lax.rem(y, 2)
    column = pl.ds(pl.multiple_of((y // 2) * 128, 128), 128)
    for dd in range(8):
        t = tok[32 * dd : 32 * dd + 32, column].astype(F32)
        t = jnp.where(half == 1, roll(t, 64), t)
        rz[dd] = jnp.where(low16, t[0:16], roll(t[16:32], 64)).astype(BF16)

    @pl.when(d == z)
    def _():
        rz[8] = rz[pl.ds(d, 1)][0]

    pl.semaphore_wait(barrier, 29 - jnp.where(d == z, 1, 0))

    for k in range(1, 8):
        to = lax.rem(d + k, 8)
        send(s1.at[to], r1.at[d], PH1, at_d(k))
    for k in range(1, 8):
        to = lax.rem(y + k, 8)
        send(ws.at[0, to], w.at[0, d, y], ST1A, at_y(k))

    @pl.when(d == z)
    def _():
        for k in range(1, 8):
            send(rz.at[lax.rem(d + k, 8)], rz.at[8], RES0, at_d(k))

    for i in range(5, 13):
        loads[i].wait()
    eye = lax.broadcasted_iota(jnp.int32, (32, 32), 0) == lax.broadcasted_iota(jnp.int32, (32, 32), 1)
    blocks = (lens[...] // BLOCK_LEN).astype(F32)
    blocks = jnp.sum(jnp.where(eye, jnp.broadcast_to(blocks, (32, 32)), 0.0), axis=1, keepdims=True)
    factor = 2.0 / (1.0 + blocks * (4.0 * BLOCK_LEN / LEN_MAX))

    def constants(layer):
        def row(ref):
            return jnp.concatenate([ref[layer, 0:1, :], ref[layer, 1:2, :]], axis=1)

        e_re, e_im = row(er), row(ei)
        rate = jnp.exp(ls[layer : layer + 1, :])
        rate = jnp.concatenate(
            [jnp.broadcast_to(rate[:, 0:1], (1, 64)), jnp.broadcast_to(rate[:, 1:2], (1, 64))], axis=1
        )
        step = rate * factor
        magnitude = jnp.exp(e_re * step)
        turned = e_im * step
        a_re = magnitude * jnp.cos(turned)
        a_im = magnitude * jnp.sin(turned)
        modulus = e_re * e_re + e_im * e_im
        b_re = ((a_re - 1.0) * e_re + a_im * e_im) / modulus
        b_im = (a_im * e_re - (a_re - 1.0) * e_im) / modulus
        u, v = st[layer, 0], st[layer, 1]
        k_re = a_re * u - a_im * v
        k_im = a_re * v + a_im * u
        rows = []
        for c in range(2):
            for g in range(2):
                slab = im[layer, c, g]
                zero = jnp.zeros((64, 16), F32)
                one = jnp.concatenate([slab, zero] if g == 0 else [zero, slab], axis=1)
                rows.append(jnp.concatenate([one] * 4, axis=1))
        hi, lo = split2(jnp.concatenate(rows, axis=0))
        in_cat = jnp.concatenate([hi, lo], axis=1)
        cols = []
        for c in range(2):
            zero = jnp.zeros((16, 64), F32)
            top = jnp.concatenate([om[layer, c, 0], zero], axis=1)
            low = jnp.concatenate([zero, om[layer, c, 1]], axis=1)
            both = jnp.concatenate([top, low], axis=0)
            cols.append(both if c == 0 else -both)
        both = jnp.concatenate(cols, axis=1)
        hi, lo = split2(jnp.concatenate([both] * 4, axis=0))
        out_cat = jnp.concatenate([hi, lo, hi], axis=1)
        direct = jnp.concatenate([skip[layer : layer + 1, :]] * 4, axis=1)
        return k_re, k_im, b_re, b_im, in_cat, out_cat, direct

    def recurrence(layer, consts, total):
        k_re, k_im, b_re, b_im, in_cat, out_cat, direct = consts
        driven = (total[0:8] * lax.rsqrt(total[8:16] / D + NORM_EPS)).astype(BF16).astype(F32)
        spread = jnp.concatenate([jnp.where(group8 == i, driven, 0.0) for i in range(4)], axis=0)
        spread = spread.astype(BF16)
        drive = lax.dot_general(
            jnp.concatenate([spread, spread], axis=1), in_cat, (((1,), (1,)), ((), ())),
            preferred_element_type=F32,
        )
        d_re, d_im = drive[:, 0:128], drive[:, 128:256]
        n_re = k_re + b_re * d_re - b_im * d_im
        n_im = k_im + b_re * d_im + b_im * d_re
        ns_ref[layer, 0] = n_re
        ns_ref[layer, 1] = n_im
        hi, lo = split2(jnp.concatenate([n_re, n_im], axis=1))
        full = lax.dot_general(
            jnp.concatenate([hi, hi, lo], axis=1), out_cat, (((1,), (1,)), ((), ())),
            preferred_element_type=F32,
        )
        value = pick4([full[8 * i : 8 * i + 8] for i in range(4)], group8) + direct * driven
        inner = 0.7978845608028654 * (value + 0.044715 * (value * value * value))
        return (value * (0.5 * (1.0 + jnp.tanh(inner)))).astype(BF16).astype(F32)

    def gather_readout(layer, value, sem):
        s2[layer] = value
        r2[layer, pl.ds(y, 1)] = value[None]
        for k in range(1, 8):
            send(s2.at[layer], r2.at[layer, y], sem, at_y(k))

    def unpack_readout(layer):
        tiles = []
        for i in range(4):
            tiles.append(
                jnp.concatenate(
                    [
                        pick4([roll(r2[layer, 4 * q + j], 32 * (j - i)) for j in range(4)], group8)
                        for q in range(2)
                    ],
                    axis=1,
                )
            )
        return jnp.concatenate(tiles, axis=0).astype(BF16)

    def near(kind, ref_of):
        mine = ref_of(d)
        for r in range(1, 4):
            to = lax.rem(x + r, 4) * 2 + core
            send(mine, mine, NEAR + 3 * kind + r - 1, {"tp": tp, "dp": to})
        send(mine, mine, PAIR + 4 * kind, {"tp": tp, "dp": x * 2 + 1 - core})

    def relay(kind, ref_of):
        for r in range(1, 4):
            ref = ref_of(lax.rem(x + 4 - r, 4) * 2 + core)
            wait_recv(ref, NEAR + 3 * kind + r - 1)
            send(ref, ref, PAIR + 4 * kind + r, {"tp": tp, "dp": x * 2 + 1 - core})

    def wait_pair(kind, ref_of):
        for r in range(4):
            wait_recv(ref_of(lax.rem(x + 4 - r, 4) * 2 + 1 - core), PAIR + 4 * kind + r)

    def near_sent(kind, ref):
        for r in range(3):
            wait_sent(ref, NEAR + 3 * kind + r)
        for r in range(4):
            wait_sent(ref, PAIR + 4 * kind + r)

    def w0(k):
        return w.at[0, k]

    def w1(k):
        return w.at[1, k]

    def wi_of(k):
        return wi.at[k]

    consts0 = constants(0)

    wait_recv(r1.at[pl.ds(0, 7)], PH1)
    value = recurrence(0, consts0, jnp.sum(r1[...], axis=0))
    gather_readout(0, value, PH2)

    wait_recv(w.at[0, 0, pl.ds(0, 7)], ST1A)
    near(0, w0)

    pack_projection(1)
    for dest in range(8):
        rows = win[1, 64 * dest : 64 * dest + 64, :].astype(F32)
        wis[dest] = jnp.concatenate([rows[16 * j : 16 * j + 16, :] for j in range(4)], axis=1).astype(BF16)
    pk[pl.ds(y, 1)] = wis[pl.ds(y, 1)]
    for k in range(1, 8):
        to = lax.rem(y + k, 8)
        send(wis.at[to], pk.at[y], ST1W, at_y(k))
    for k in range(1, 8):
        to = lax.rem(y + k, 8)
        send(ws.at[1, to], w.at[1, d, y], ST1B, at_y(k))
    own_gain = gain[1:2, column]
    gb[pl.ds(d, 1)] = jnp.where(half == 1, roll(own_gain, 64), own_gain)[None]
    for k in range(1, 8):
        send(gb.at[d], gb.at[d], GAIN, at_d(k))

    wait_recv(r2.at[0, pl.ds(0, 7)], PH2)
    piece = unpack_readout(0)
    relay(0, w0)
    wait_pair(0, w0)
    for k in range(8):
        s3[k] = jnp.dot(
            piece, w[0, k].reshape(256, 128), preferred_element_type=F32
        ).astype(BF16)
    for k in range(1, 8):
        send(s3.at[lax.rem(z + k, 8)], r3.at[z], PH3, at_z(k))
    r3[pl.ds(z, 1)] = s3[pl.ds(z, 1)]

    wait_recv(pk.at[pl.ds(0, 7)], ST1W)
    group16 = groups4(16)
    for j in range(4):
        cols = []
        for q in range(2):
            cols.append(
                pick4([roll(pk[4 * q + g].astype(F32), 32 * (g - j)) for g in range(4)], group16)
            )
        wi[pl.ds(d, 1), 16 * j : 16 * j + 16, :] = jnp.concatenate(cols, axis=1).astype(BF16)[None]
    near(2, wi_of)
    wait_recv(w.at[1, 0, pl.ds(0, 7)], ST1B)
    near(1, w1)

    @pl.when(d != z)
    def _():
        wait_recv(rz.at[8], RES0)

    def gated(parts, residual):
        top, low = parts[0:16], parts[16:32]
        linear = jnp.where(low16, top, roll(low, 64))
        gate_sum = jnp.where(low16, roll(top, 64), low)
        return (residual + linear * (1.0 / (1.0 + jnp.exp(-gate_sum)))).astype(BF16)

    residual0 = rz[8].astype(F32)
    wait_recv(r3.at[pl.ds(0, 7)], PH3)
    own = gated(jnp.sum(r3[...].astype(F32), axis=0), residual0)
    m0[...] = own
    r4[pl.ds(z, 1)] = own[None]
    for k in range(1, 8):
        send(m0, r4.at[z], PH4, at_z(k))

    @pl.when(d != z)
    def _():
        send(m0, rz1, RES1, {"tp": d * 8 + y, "dp": z})

    @pl.when(d == z)
    def _():
        rz1[...] = own

    relay(2, wi_of)
    relay(1, w1)
    consts1 = constants(1)
    wait_recv(gb.at[pl.ds(0, 7)], GAIN)
    low1 = low_half(1)
    gains = [jnp.where(low1, gb[2 * q], roll(gb[2 * q + 1], 64)) for q in range(4)]
    wait_pair(2, wi_of)

    wait_recv(r4.at[pl.ds(0, 7)], PH4)
    tiles = []
    sq = jnp.zeros((32, 1), F32)
    for q in range(4):
        a, b = r4[2 * q].astype(F32), r4[2 * q + 1].astype(F32)
        cur = jnp.concatenate(
            [jnp.where(low16, a, roll(b, 64)), jnp.where(low16, roll(a, 64), b)], axis=0
        )
        sq = sq + jnp.sum(cur * cur, axis=1, keepdims=True)
        tiles.append((cur * gains[q]).astype(BF16))
    part = jnp.dot(
        jnp.concatenate(tiles, axis=1), wi[...].reshape(512, 256), preferred_element_type=F32
    )
    squares = pick4([jnp.broadcast_to(sq[8 * i : 8 * i + 8, :], (8, 128)) for i in range(4)], group8)
    for q in range(2):
        rows = [part[8 * i : 8 * i + 8, 128 * q : 128 * q + 128] for i in range(4)]
        for j in range(4):
            s5[4 * q + j, 0:8, :] = pick4([roll(rows[i], 32 * (i - j)) for i in range(4)], group8)
            s5[4 * q + j, 8:16, :] = squares
    for k in range(1, 8):
        send(s5.at[lax.rem(y + k, 8)], r5.at[y], PH5, at_y(k))
    r5[pl.ds(y, 1)] = s5[pl.ds(y, 1)]
    wait_recv(r5.at[pl.ds(0, 7)], PH5)
    value = recurrence(1, consts1, jnp.sum(r5[...], axis=0))
    gather_readout(1, value, PH6)
    wait_pair(1, w1)

    @pl.when(d != z)
    def _():
        wait_recv(rz1, RES1)

    wait_recv(r2.at[1, pl.ds(0, 7)], PH6)
    piece = unpack_readout(1)
    for k in range(8):
        s7[k] = jnp.dot(
            piece, w[1, k].reshape(256, 128), preferred_element_type=F32
        ).astype(BF16)
    for k in range(8):
        @pl.when(jnp.logical_not(jnp.logical_and(d == k, d == z)))
        def _(k=k):
            send(s7.at[k], r7.at[z], PH7, {"tp": d * 8 + y, "dp": k})

    @pl.when(d == z)
    def _():
        r7[pl.ds(z, 1)] = s7[pl.ds(z, 1)]
        wait_recv(r7.at[pl.ds(0, 7)], PH7)

    @pl.when(d != z)
    def _():
        wait_recv(r7, PH7)

    own = gated(jnp.sum(r7[...].astype(F32), axis=0), rz1[...].astype(F32))

    odd = lax.rem(y + z, 2)

    @pl.when(odd == 0)
    def _():
        oa[pl.ds(y, 1), pl.ds(z // 2, 1)] = own[None, None]
        for k in range(1, 8):
            send(oa.at[y, z // 2], oa.at[y, z // 2], PH8, at_z(k))

    @pl.when(odd == 1)
    def _():
        ob[pl.ds(z, 1), pl.ds(y // 2, 1)] = own[None, None]
        for k in range(1, 8):
            send(ob.at[z, y // 2], ob.at[z, y // 2], PH8, at_y(k))

    wait_recv(r4.at[pl.ds(0, 7)], PH8)
    for k in range(1, 8):
        send(oa.at[y], oa.at[y], PH9A, at_y(k))
        send(ob.at[z], ob.at[z], PH9B, at_z(k))
    wait_recv(oa.at[pl.ds(0, 7)], PH9A)
    wait_recv(ob.at[pl.ds(0, 7)], PH9B)
    for zz in range(8):
        for q in range(4):
            a, b = [
                (oa[yy, zz // 2] if (yy + zz) % 2 == 0 else ob[zz, yy // 2]).astype(F32)
                for yy in (2 * q, 2 * q + 1)
            ]
            mixed_ref[32 * zz : 32 * zz + 32, 128 * q : 128 * q + 128] = jnp.concatenate(
                [jnp.where(low16, a, roll(b, 64)), jnp.where(low16, roll(a, 64), b)], axis=0
            ).astype(BF16)

    wait_sent(s1.at[pl.ds(0, 7)], PH1)
    wait_sent(ws.at[0, pl.ds(0, 7)], ST1A)
    wait_sent(ws.at[1, pl.ds(0, 7)], ST1B)
    wait_sent(wis.at[pl.ds(0, 7)], ST1W)
    wait_sent(gb.at[pl.ds(0, 7)], GAIN)
    wait_sent(r2.at[0, pl.ds(0, 7)], PH2)
    wait_sent(r2.at[1, pl.ds(0, 7)], PH6)
    wait_sent(s3.at[pl.ds(0, 7)], PH3)
    wait_sent(r4.at[pl.ds(0, 7)], PH4)
    wait_sent(s5.at[pl.ds(0, 7)], PH5)
    wait_sent(r4.at[pl.ds(0, 7)], PH8)
    wait_sent(oa.at[pl.ds(0, 7)], PH9A)
    wait_sent(ob.at[pl.ds(0, 7)], PH9B)
    near_sent(0, w.at[0, 0])
    near_sent(1, w.at[1, 0])
    near_sent(2, wi.at[0])

    @pl.when(d == z)
    def _():
        wait_sent(rz.at[pl.ds(0, 7)], RES0)
        wait_sent(s7.at[pl.ds(0, 7)], PH7)

    @pl.when(d != z)
    def _():
        wait_sent(m0, RES1)
        wait_sent(s7, PH7)


def body(tokens, lengths, norm_gain, w_in, log_step, eig_re, eig_im, in_mat, output_matrices, skip,
         w_glu, w_gate, state):
    args = (tokens, lengths.reshape(1, 32), norm_gain, w_in, log_step, eig_re, eig_im, in_mat,
            output_matrices, skip, w_glu, w_gate, state)
    return pl.pallas_call(
        kernel,
        name="decode",
        out_shape=(
            jax.ShapeDtypeStruct((256, 512), BF16),
            jax.ShapeDtypeStruct((2, 2, 32, 128), F32),
        ),
        in_specs=[pl.BlockSpec(memory_space=pl.ANY)] * 13,
        out_specs=(pl.BlockSpec(memory_space=pltpu.VMEM),) * 2,
        scratch_shapes=[pltpu.VMEM(a.shape, a.dtype) for a in args]
        + [
            pltpu.VMEM((8, 16, 128), F32),
            pltpu.VMEM((8, 16, 128), F32),
            pltpu.VMEM((2, 8, 32, 128), BF16),
            pltpu.VMEM((2, 8, 8, 32, 128), BF16),
            pltpu.VMEM((8, 16, 128), BF16),
            pltpu.VMEM((8, 16, 128), BF16),
            pltpu.VMEM((8, 64, 256), BF16),
            pltpu.VMEM((8, 1, 128), F32),
            pltpu.VMEM((9, 16, 128), BF16),
            pltpu.VMEM((16, 128), BF16),
            pltpu.VMEM((2, 8, 128), F32),
            pltpu.VMEM((2, 8, 8, 128), F32),
            pltpu.VMEM((8, 32, 128), BF16),
            pltpu.VMEM((8, 32, 128), BF16),
            pltpu.VMEM((8, 16, 128), BF16),
            pltpu.VMEM((16, 128), BF16),
            pltpu.VMEM((8, 16, 128), F32),
            pltpu.VMEM((8, 16, 128), F32),
            pltpu.VMEM((8, 32, 128), BF16),
            pltpu.VMEM((8, 32, 128), BF16),
            pltpu.VMEM((8, 4, 16, 128), BF16),
            pltpu.VMEM((8, 4, 16, 128), BF16),
            pltpu.SemaphoreType.DMA((13,)),
            pltpu.SemaphoreType.DMA((COUNT,)),
            pltpu.SemaphoreType.DMA((COUNT,)),
        ],
        compiler_params=pltpu.CompilerParams(collective_id=0, has_side_effects=True),
    )(*args)


def solution(mesh):
    placed = (
        P(None, "dp"),
        P("dp"),
        P(None, "dp"),
        P(None, "dp", "tp"),
        P(None, "tp"),
        P(None, "tp", None),
        P(None, "tp", None),
        P(None, None, "tp", None, None),
        P(None, None, "tp", None, None),
        P(None, "tp"),
        P(None, "tp", "dp"),
        P(None, "tp", "dp"),
        P(None, None, "dp", "tp"),
    )
    return jax.shard_map(
        body,
        mesh=mesh,
        in_specs=placed,
        out_specs=(P(None, "dp"), P(None, None, "dp", "tp")),
        check_vma=False,
    )
```

time: 179 us -> 70 us (0.39); the launches traced: 177 us -> 69.5 us
  waiting for transfers between devices: 93.9 us -> 0 us
  Pallas kernels: 0 us -> 64 us
  starting transfers between devices: 57 us -> 0 us
  local copies, waits for them, and re-layouts: 17.9 us -> 4.87 us
  other arithmetic: 3.67 us -> 0 us
  matrix products: 3.06 us -> 0 us
    all_to_all x8 -> x0, waiting for transfers between devices: 93.9 us -> none  [the longest x4 61.2 us: sent_and_summed(): lax.all_to_all(pieces, axis, split_axis=0, concat_axis=0, tiled=True)]
    pallas_call x0 -> x1, Pallas kernels: none -> 64 us  [body(): pl.pallas_call(kernel, name='decode', out_shape=(jax.ShapeDtypeStruct((25...]
    all_to_all x8 -> x0, starting transfers between devices: 57 us -> none  [the longest x4 33.5 us: sent_and_summed(): lax.all_to_all(pieces, axis, split_axis=0, concat_axis=0, tiled=True)]
    unnamed x36 -> x8, local copies, waits for them, and re-layouts: 9.72 us -> 4.87 us
    transpose x2 -> x0, local copies, waits for them, and re-layouts: 3.18 us -> none  [split_up(): return jnp.moveaxis(array.reshape(*before, length, -1, *after), dim, 0)]
    dot_general x14 -> x0, matrix products: 3.06 us -> none  [the longest x2 0.61 us: body(): jnp.dot(scaled, w_in[layer_index], preferred_element_type=jnp.float32)]
  transfers between devices with their start and end apart: 8 -> 0, of which waited for: 8 -> 0; matrix products, arithmetic and copies ran while one was open for 1% -> 0% of each run, Pallas kernels for 0% -> 0%
where the time goes in v1:
time: 70 us; the launch traced here: 69.5 us
  Pallas kernels  64 us (91%)
  local copies, waits for them, and re-layouts  4.87 us (7%)
    pallas_call x1, Pallas kernels, body(): pl.pallas_call(kernel, name='decode', out_shape=(jax.ShapeDtypeStruct((25...  64 us
    unnamed x8, local copies, waits for them, and re-layouts  4.87 us

profile of v1, /device:TPU:1, one launch (start us, length us, event | category | flops | bytes accessed | tf_op | source)
XLA Modules:
  0.0 69.5 jit_solution(16881925357262912611)
XLA Ops:
  0.6 0.0 copy-start
  0.6 1.7 %copy.15.win_h = bf16[2,512,32]{2,1,0:T(8,128)(2,1)} copy(bf16[2,512,32]{1,2,0:T(8,128)(2,1)} %param.16) | data formatting | bytes 131072 | tf_op args[3]
  2.4 0.0 copy-done
  2.4 0.8 %copy.16.im_h = f32[2,2,2,64,16]{4,3,2,1,0:T(8,128)} copy(f32[2,2,2,64,16]{3,4,2,1,0:T(8,128)S(1)} %copy-done) | data formatting | bytes 65536 | tf_op args[7]
  3.2 64.0 %decode.1 = (bf16[256,512]{1,0:T(8,128)(2,1)}, f32[2,2,32,128]{3,2,1,0:T(8,128)}) custom-call(bf16[256,512]{1,0:T(8,128)(2,1)} %tok_h.1, s32[1,32]{1,0:T(1,128)} %bitcast.1, f32[2,512]{1,0:T(2,128)} %gain_h.1, bf16[2,512,32]{2,1,0:T(8,128)(2,1)} %copy.15.win_h, f32[2,2]{1,0:T(2,128)} %ls_h.1, f32[2,2,64]{2,1,0:T(2,128)} %er_h.1, f32[2,2,64]{2,1,0:T(2,128)} %ei_h.1, ...), custom_call_target="tpu_custom_call" | custom-call | tf_op jit(solution)/shard_map/decode/pallas_call | solution.py:482
  67.1 0.0 copy-start.1
  67.1 1.7 %copy.19 = bf16[256,512]{1,0:T(8,128)(2,1)} copy(bf16[256,512]{1,0:T(8,128)(2,1)} %get-tuple-element.4) | data formatting | bytes 524288
  68.9 0.0 copy-done.1
  68.9 0.6 copy.20
Async XLA Ops:
  0.6 1.7 %copy-start = (f32[2,2,2,64,16]{3,4,2,1,0:T(8,128)S(1)}, f32[2,2,2,64,16]{3,4,2,1,0:T(8,128)}, u32[]{:S(2)}) copy-start(f32[2,2,2,64,16]{3,4,2,1,0:T(8,128)} %param.20) | copy-start | bytes 98308
  67.1 1.7 %copy-start.1 = (f32[2,2,32,128]{3,2,1,0:T(8,128)S(1)}, f32[2,2,32,128]{3,2,1,0:T(8,128)}, u32[]{:S(2)}) copy-start(f32[2,2,32,128]{3,2,1,0:T(8,128)} %get-tuple-element.5) | copy-start | bytes 196612

commit v2 on v1

v2 whole, which is shorter than its diff:
```python
import jax
import jax.numpy as jnp
from jax import lax
from jax.experimental import pallas as pl
from jax.experimental.pallas import tpu as pltpu
from jax.sharding import PartitionSpec as P

D = 4096
LEN_MAX = 4096
BLOCK_LEN = 256
NORM_EPS = 1e-06
MESH = pl.DeviceIdType.MESH
NT = (((1,), (1,)), ((), ()))
F32 = jnp.float32
BF16 = jnp.bfloat16

(PH1, RES0, PH2, ST1B, ST1W, PH3, PH4, RES1, PH5, PH6, PH7, PH9A, PH9B, GAIN) = range(14)
NEAR = 14
PAIR = NEAR + 9
FAR = PAIR + 12
LASTZ = FAR + 7
LASTY = LASTZ + 7
COUNT = LASTY + 7
NEAREST = (1, 7, 2, 6, 3, 5, 4)
FARTHEST = (4, 3, 5, 2, 6, 1, 7)


def roll(x, amount):
    amount = amount % 128
    return x if amount == 0 else pltpu.roll(x, amount, 1)


def groups4(rows):
    return lax.broadcasted_iota(jnp.int32, (rows, 128), 1) // 32


def low_half(rows):
    return lax.broadcasted_iota(jnp.int32, (rows, 128), 1) < 64


def pick4(parts, group):
    out = parts[3]
    for i in (2, 1, 0):
        out = jnp.where(group == i, parts[i], out)
    return out


def split2(x):
    hi = x.astype(BF16)
    lo = (x - hi.astype(F32)).astype(BF16)
    return hi, lo


def kernel(
    tok_h, len_h, gain_h, win_h, ls_h, er_h, ei_h, im_h, om_h, skip_h, glu_h, gate_h, st_h,
    mixed_ref, ns_ref,
    tok, lens, gain, win, ls, er, ei, im, om, skip, glu, gate, st,
    s1, r1, ws, w, wis, pk, wi, gb, rz, rz1, s2, r2, s3, r3, r4, m0, s5, r5, s7, r7, oa, ob,
    lsem, ss, rs,
):
    tp = lax.axis_index("tp")
    d = lax.axis_index("dp")
    z = tp // 8
    y = lax.rem(tp, 8)
    x = d // 2
    core = lax.rem(d, 2)

    def at_y(k):
        return {"tp": z * 8 + lax.rem(y + k, 8), "dp": d}

    def at_z(k):
        return {"tp": lax.rem(z + k, 8) * 8 + y, "dp": d}

    def at_d(k):
        return {"tp": tp, "dp": lax.rem(d + k, 8)}

    def send(src, dst, sem, dev, rsem=None):
        pltpu.make_async_remote_copy(
            src_ref=src,
            dst_ref=dst,
            send_sem=ss.at[sem],
            recv_sem=rs.at[sem if rsem is None else rsem],
            device_id=dev,
            device_id_type=MESH,
        ).start()

    def wait_recv(ref, sem):
        with jax.named_scope(f"recv{sem}"):
            pltpu.make_async_copy(ref, ref, rs.at[sem]).wait()

    def wait_sent(ref, sem):
        pltpu.make_async_copy(ref, ref, ss.at[sem]).wait()

    def pass_on(k):
        block = w.at[0, d, lax.rem(y + 8 - k, 8)]
        if k:
            wait_recv(block, FAR + k - 1)
        for r in range(1, 4):
            to = lax.rem(x + r, 4) * 2 + core
            send(block, block, NEAR + r - 1, {"tp": tp, "dp": to})

    hbm = (tok_h, win_h, gain_h, glu_h, gate_h, len_h, ls_h, er_h, ei_h, im_h, om_h, skip_h, st_h)
    vmem = (tok, win, gain, glu, gate, lens, ls, er, ei, im, om, skip, st)
    loads = [pltpu.make_async_copy(a, b, lsem.at[i]) for i, (a, b) in enumerate(zip(hbm, vmem))]
    for copy in loads[:3]:
        copy.start()

    barrier = pltpu.get_barrier_semaphore()
    for at in (at_y, at_z, at_d):
        for k in FARTHEST:
            pl.semaphore_signal(barrier, inc=1, device_id=at(k), device_id_type=MESH)
    for copy in loads[3:]:
        copy.start()

    def fold_low(t):
        return jnp.where(low16, t[0:16], roll(t[16:32], 64))

    def fold_high(t):
        return jnp.where(low16, roll(t[0:16], 64), t[16:32])

    def unfold(a, b):
        return jnp.concatenate(
            [jnp.where(low16, a, roll(b, 64)), jnp.where(low16, roll(a, 64), b)], axis=0
        )

    group8 = groups4(8)
    low16 = low_half(16)
    low32 = low_half(32)
    low128 = low_half(128)

    with jax.named_scope("load0"):
        for i in range(3):
            loads[i].wait()
    for dd in range(8):
        t = tok[32 * dd : 32 * dd + 32, :].astype(F32)
        scaled = (t * gain[0:1, :]).astype(BF16)
        part = lax.dot_general(scaled, win[0], NT, preferred_element_type=F32)
        sq = jnp.sum(t * t, axis=1, keepdims=True)
        packed = jnp.concatenate([part[8 * i : 8 * i + 8, :] for i in range(4)], axis=1)
        spread = pick4([jnp.broadcast_to(sq[8 * i : 8 * i + 8, :], (8, 128)) for i in range(4)], group8)
        s1[dd] = jnp.concatenate([packed, spread], axis=0).astype(BF16)
    r1[pl.ds(d, 1)] = s1[pl.ds(d, 1)]

    loads[3].wait()
    loads[4].wait()

    def pack_projection(layer):
        for q in range(4):
            g = glu[layer, :, 128 * q : 128 * q + 128].astype(F32)
            t = gate[layer, :, 128 * q : 128 * q + 128].astype(F32)
            ws[layer, 2 * q] = jnp.where(low32, g, roll(t, 64)).astype(BF16)
            ws[layer, 2 * q + 1] = jnp.where(low32, roll(g, 64), t).astype(BF16)
        w[layer, pl.ds(d, 1), pl.ds(y, 1)] = ws[layer, pl.ds(y, 1)][None]

    pack_projection(0)

    half = lax.rem(y, 2)
    column = pl.ds(pl.multiple_of((y // 2) * 128, 128), 128)
    for dd in range(8):
        t = tok[32 * dd : 32 * dd + 32, column].astype(F32)
        t = jnp.where(half == 1, roll(t, 64), t)
        rz[dd] = fold_low(t).astype(BF16)

    @pl.when(d == z)
    def _():
        rz[8] = rz[pl.ds(d, 1)][0]

    with jax.named_scope("entry"):
        pl.semaphore_wait(barrier, 21)

    for k in FARTHEST:
        to = lax.rem(d + k, 8)
        send(s1.at[to], r1.at[d], PH1, at_d(k))
    for k in FARTHEST:
        to = lax.rem(y + k, 8)
        send(ws.at[0, to], w.at[0, d, y], FAR + k - 1, at_y(k))
    pass_on(0)

    @pl.when(d == z)
    def _():
        for k in FARTHEST:
            send(rz.at[lax.rem(d + k, 8)], rz.at[8], RES0, at_d(k))

    for i in range(5, 13):
        loads[i].wait()
    eye = lax.broadcasted_iota(jnp.int32, (32, 32), 0) == lax.broadcasted_iota(jnp.int32, (32, 32), 1)
    blocks = (lens[...] // BLOCK_LEN).astype(F32)
    blocks = jnp.sum(jnp.where(eye, jnp.broadcast_to(blocks, (32, 32)), 0.0), axis=1, keepdims=True)
    factor = 2.0 / (1.0 + blocks * (4.0 * BLOCK_LEN / LEN_MAX))

    def by_group(slabs, sign):
        zero = jnp.zeros((16, 64), F32)
        cols = []
        for c in range(2):
            top = jnp.concatenate([slabs[2 * c], zero], axis=1)
            low = jnp.concatenate([zero, slabs[2 * c + 1]], axis=1)
            both = jnp.concatenate([top, low], axis=0)
            cols.append(both if c == 0 else sign * both)
        return jnp.concatenate([jnp.concatenate(cols, axis=1)] * 4, axis=0)

    def constants(layer):
        def row(ref):
            return jnp.concatenate([ref[layer, 0:1, :], ref[layer, 1:2, :]], axis=1)

        e_re, e_im = row(er), row(ei)
        rate = jnp.exp(ls[layer : layer + 1, :])
        rate = jnp.concatenate(
            [jnp.broadcast_to(rate[:, 0:1], (1, 64)), jnp.broadcast_to(rate[:, 1:2], (1, 64))], axis=1
        )
        step = rate * factor
        magnitude = jnp.exp(e_re * step)
        turned = e_im * step
        a_re = magnitude * jnp.cos(turned)
        a_im = magnitude * jnp.sin(turned)
        modulus = e_re * e_re + e_im * e_im
        b_re = ((a_re - 1.0) * e_re + a_im * e_im) / modulus
        b_im = (a_im * e_re - (a_re - 1.0) * e_im) / modulus
        u, v = st[layer, 0], st[layer, 1]
        k_re = a_re * u - a_im * v
        k_im = a_re * v + a_im * u
        hi, lo = split2(by_group([im[layer, c, g] for c in range(2) for g in range(2)], 1.0))
        in_cat = jnp.concatenate([hi, lo], axis=0)
        hi, lo = split2(by_group([om[layer, c, g] for c in range(2) for g in range(2)], -1.0))
        out_cat = jnp.concatenate([hi, lo, hi], axis=1)
        direct = jnp.concatenate([skip[layer : layer + 1, :]] * 4, axis=1)
        return k_re, k_im, b_re, b_im, in_cat, out_cat, direct

    def recurrence(layer, consts, total):
        k_re, k_im, b_re, b_im, in_cat, out_cat, direct = consts
        driven = (total[0:8] * lax.rsqrt(total[8:16] / D + NORM_EPS)).astype(BF16).astype(F32)
        spread = jnp.concatenate([jnp.where(group8 == i, driven, 0.0) for i in range(4)], axis=0)
        spread = spread.astype(BF16)
        drive = lax.dot_general(
            jnp.concatenate([spread, spread], axis=1), in_cat, (((1,), (0,)), ((), ())),
            preferred_element_type=F32,
        )
        d_re, d_im = drive[:, 0:128], drive[:, 128:256]
        n_re = k_re + b_re * d_re - b_im * d_im
        n_im = k_im + b_re * d_im + b_im * d_re
        ns_ref[layer, 0] = n_re
        ns_ref[layer, 1] = n_im
        hi, lo = split2(jnp.concatenate([n_re, n_im], axis=1))
        full = lax.dot_general(
            jnp.concatenate([hi, hi, lo], axis=1), out_cat, NT, preferred_element_type=F32
        )
        value = pick4([full[8 * i : 8 * i + 8] for i in range(4)], group8) + direct * driven
        inner = 0.7978845608028654 * (value + 0.044715 * (value * value * value))
        return (value * (0.5 * (1.0 + jnp.tanh(inner)))).astype(BF16)

    def gather_readout(layer, value, sem):
        s2[layer] = value
        r2[layer, pl.ds(y, 1)] = value[None]
        for k in FARTHEST:
            send(s2.at[layer], r2.at[layer, y], sem, at_y(k))

    def unpack_readout(layer):
        got = [r2[layer, j].astype(F32) for j in range(8)]
        tiles = []
        for i in range(4):
            tiles.append(
                jnp.concatenate(
                    [
                        pick4([roll(got[4 * q + j], 32 * (j - i)) for j in range(4)], group8)
                        for q in range(2)
                    ],
                    axis=1,
                )
            )
        return jnp.concatenate(tiles, axis=0).astype(BF16)

    def near(kind, ref_of):
        mine = ref_of(d)
        for r in range(1, 4):
            to = lax.rem(x + r, 4) * 2 + core
            send(mine, mine, NEAR + 3 * kind + r - 1, {"tp": tp, "dp": to})
        to_pair(kind, ref_of)

    def to_pair(kind, ref_of):
        send(ref_of(d), ref_of(d), PAIR + 4 * kind, {"tp": tp, "dp": x * 2 + 1 - core})

    def relay(kind, ref_of):
        for r in range(1, 4):
            ref = ref_of(lax.rem(x + 4 - r, 4) * 2 + core)
            wait_recv(ref, NEAR + 3 * kind + r - 1)
            send(ref, ref, PAIR + 4 * kind + r, {"tp": tp, "dp": x * 2 + 1 - core})

    def wait_pair(kind, ref_of):
        for r in range(4):
            wait_recv(ref_of(lax.rem(x + 4 - r, 4) * 2 + 1 - core), PAIR + 4 * kind + r)

    def near_sent(kind, ref):
        for r in range(3):
            wait_sent(ref, NEAR + 3 * kind + r)
        for r in range(4):
            wait_sent(ref, PAIR + 4 * kind + r)

    def w0(k):
        return w.at[0, k]

    def w1(k):
        return w.at[1, k]

    def wi_of(k):
        return wi.at[k]

    consts0 = constants(0)

    for k in NEAREST[:4]:
        pass_on(k)
    wait_recv(r1.at[pl.ds(0, 7)], PH1)
    value = recurrence(0, consts0, jnp.sum(r1[...].astype(F32), axis=0))
    gather_readout(0, value, PH2)
    for k in NEAREST[4:]:
        pass_on(k)
    to_pair(0, w0)

    pack_projection(1)
    for q in range(4):
        t = win[1, :, 128 * q : 128 * q + 128].astype(F32)
        wis[2 * q] = fold_low(t).astype(BF16)
        wis[2 * q + 1] = fold_high(t).astype(BF16)
    pk[pl.ds(y, 1)] = wis[pl.ds(y, 1)]
    for k in FARTHEST:
        to = lax.rem(y + k, 8)
        send(wis.at[to], pk.at[y], ST1W, at_y(k))
    for k in FARTHEST:
        to = lax.rem(y + k, 8)
        send(ws.at[1, to], w.at[1, d, y], ST1B, at_y(k))
    own_gain = gain[1:2, column]
    gb[pl.ds(d, 1)] = jnp.where(half == 1, roll(own_gain, 64), own_gain)[None]
    for k in FARTHEST:
        send(gb.at[d], gb.at[d], GAIN, at_d(k))

    relay(0, w0)
    wait_recv(r2.at[0, pl.ds(0, 7)], PH2)
    piece = unpack_readout(0)
    wait_pair(0, w0)
    for k in range(8):
        s3[k] = jnp.dot(
            piece, w[0, k].reshape(256, 128), preferred_element_type=F32
        ).astype(BF16)
    for k in FARTHEST:
        send(s3.at[lax.rem(z + k, 8)], r3.at[z], PH3, at_z(k))
    r3[pl.ds(z, 1)] = s3[pl.ds(z, 1)]

    wait_recv(pk.at[pl.ds(0, 7)], ST1W)
    for j in range(4):
        rows = unfold(pk[j].astype(F32), pk[4 + j].astype(F32)).astype(BF16)
        wi[pl.ds(d, 1), 32 * j : 32 * j + 32, :] = rows[None]
    near(2, wi_of)
    wait_recv(w.at[1, 0, pl.ds(0, 7)], ST1B)
    near(1, w1)

    @pl.when(d != z)
    def _():
        wait_recv(rz.at[8], RES0)

    def gated(parts, residual):
        linear, gate_sum = fold_low(parts), fold_high(parts)
        return (residual + linear * (1.0 / (1.0 + jnp.exp(-gate_sum)))).astype(BF16)

    residual0 = rz[8].astype(F32)
    wait_recv(r3.at[pl.ds(0, 7)], PH3)
    own = gated(jnp.sum(r3[...].astype(F32), axis=0), residual0)
    m0[...] = own
    r4[pl.ds(z, 1)] = own[None]
    for k in FARTHEST:
        send(m0, r4.at[z], PH4, at_z(k))

    alone = jnp.logical_and(z == 0, d == 0)

    @pl.when(jnp.logical_not(alone))
    def _():
        send(m0, rz1, RES1, {"tp": lax.rem(d + z, 8) * 8 + y, "dp": z})

    @pl.when(alone)
    def _():
        rz1[...] = own

    relay(2, wi_of)
    relay(1, w1)
    consts1 = constants(1)
    wait_recv(gb.at[pl.ds(0, 7)], GAIN)
    low1 = low_half(1)
    gains = [jnp.where(low1, gb[2 * q], roll(gb[2 * q + 1], 64)) for q in range(4)]
    wait_pair(2, wi_of)
    cols = []
    for q in range(4):
        a, b = wi[2 * q].astype(F32), wi[2 * q + 1].astype(F32)
        cols.append(
            jnp.concatenate(
                [jnp.where(low128, a, roll(b, 64)), jnp.where(low128, roll(a, 64), b)], axis=0
            ).astype(BF16)
        )
    win_t = jnp.concatenate(cols, axis=1)

    wait_recv(r4.at[pl.ds(0, 7)], PH4)
    tiles = []
    sq = jnp.zeros((32, 1), F32)
    for q in range(4):
        cur = unfold(r4[2 * q].astype(F32), r4[2 * q + 1].astype(F32))
        sq = sq + jnp.sum(cur * cur, axis=1, keepdims=True)
        tiles.append((cur * gains[q]).astype(BF16))
    part = lax.dot_general(jnp.concatenate(tiles, axis=1), win_t, NT, preferred_element_type=F32)
    squares = pick4([jnp.broadcast_to(sq[8 * i : 8 * i + 8, :], (8, 128)) for i in range(4)], group8)
    for q in range(2):
        rows = [part[8 * i : 8 * i + 8, 128 * q : 128 * q + 128] for i in range(4)]
        for j in range(4):
            packed = pick4([roll(rows[i], 32 * (i - j)) for i in range(4)], group8)
            s5[4 * q + j] = jnp.concatenate([packed, squares], axis=0).astype(BF16)
    for k in FARTHEST:
        send(s5.at[lax.rem(y + k, 8)], r5.at[y], PH5, at_y(k))
    r5[pl.ds(y, 1)] = s5[pl.ds(y, 1)]
    wait_recv(r5.at[pl.ds(0, 7)], PH5)
    value = recurrence(1, consts1, jnp.sum(r5[...].astype(F32), axis=0))
    gather_readout(1, value, PH6)
    wait_pair(1, w1)

    @pl.when(jnp.logical_or(z != 0, d != 0))
    def _():
        wait_recv(rz1, RES1)

    wait_recv(r2.at[1, pl.ds(0, 7)], PH6)
    piece = unpack_readout(1)
    for k in range(8):
        s7[k] = jnp.dot(
            piece, w[1, k].reshape(256, 128), preferred_element_type=F32
        ).astype(BF16)
    keeps = z == lax.rem(2 * d, 8)
    for k in (0, *FARTHEST):
        to = lax.rem(d + k, 8)
        dev = {"tp": lax.rem(d + to, 8) * 8 + y, "dp": to}
        if k:
            send(s7.at[to], r7.at[z], PH7, dev)
        else:

            @pl.when(jnp.logical_not(keeps))
            def _(to=to, dev=dev):
                send(s7.at[to], r7.at[z], PH7, dev)

    wait_sent(s1.at[pl.ds(0, 7)], PH1)
    for k in range(7):
        wait_sent(ws.at[0, 0], FAR + k)
    wait_sent(ws.at[1, pl.ds(0, 7)], ST1B)
    wait_sent(wis.at[pl.ds(0, 7)], ST1W)
    wait_sent(gb.at[pl.ds(0, 7)], GAIN)
    wait_sent(r2.at[0, pl.ds(0, 7)], PH2)
    wait_sent(r2.at[1, pl.ds(0, 7)], PH6)
    wait_sent(s3.at[pl.ds(0, 7)], PH3)
    wait_sent(r4.at[pl.ds(0, 7)], PH4)
    wait_sent(s5.at[pl.ds(0, 7)], PH5)
    near_sent(0, w.at[0, 0])
    near_sent(1, w.at[1, 0])
    near_sent(2, wi.at[0])

    @pl.when(d == z)
    def _():
        wait_sent(rz.at[pl.ds(0, 7)], RES0)

    @pl.when(jnp.logical_or(z != 0, d != 0))
    def _():
        wait_sent(m0, RES1)

    @pl.when(keeps)
    def _():
        r7[pl.ds(z, 1)] = s7[pl.ds(d, 1)]
        wait_recv(r7.at[pl.ds(0, 7)], PH7)

    @pl.when(jnp.logical_not(keeps))
    def _():
        wait_recv(r7, PH7)

    own = gated(jnp.sum(r7[...].astype(F32), axis=0), rz1[...].astype(F32))

    odd = lax.rem(y + z, 2)

    def forward_a(zz):
        for k in FARTHEST:
            send(oa.at[y, zz // 2], oa.at[y, zz // 2], PH9A, at_y(k))

    def forward_b(yy):
        for k in FARTHEST:
            send(ob.at[z, yy // 2], ob.at[z, yy // 2], PH9B, at_z(k))

    def from_z(k):
        zz = lax.rem(z + 8 - k, 8)
        wait_recv(oa.at[y, zz // 2], LASTZ + k - 1)
        forward_a(zz)

    def from_y(k):
        yy = lax.rem(y + 8 - k, 8)
        wait_recv(ob.at[z, yy // 2], LASTY + k - 1)
        forward_b(yy)

    @pl.when(odd == 0)
    def _():
        oa[pl.ds(y, 1), pl.ds(z // 2, 1)] = own[None, None]
        for k in FARTHEST:
            send(oa.at[y, z // 2], oa.at[y, z // 2], LASTZ + k - 1, at_z(k))
        forward_a(z)
        for k in NEAREST:
            (from_z if k % 2 == 0 else from_y)(k)

    @pl.when(odd == 1)
    def _():
        ob[pl.ds(z, 1), pl.ds(y // 2, 1)] = own[None, None]
        for k in FARTHEST:
            send(ob.at[z, y // 2], ob.at[z, y // 2], LASTY + k - 1, at_y(k))
        forward_b(y)
        for k in NEAREST:
            (from_y if k % 2 == 0 else from_z)(k)

    wait_recv(oa.at[pl.ds(0, 7)], PH9A)
    wait_recv(ob.at[pl.ds(0, 7)], PH9B)
    for zz in range(8):
        rows = pl.ds(pl.multiple_of(lax.rem(zz + 8 - d, 8) * 32, 32), 32)
        for q in range(4):
            a, b = [
                (oa[yy, zz // 2] if (yy + zz) % 2 == 0 else ob[zz, yy // 2]).astype(F32)
                for yy in (2 * q, 2 * q + 1)
            ]
            mixed_ref[rows, 128 * q : 128 * q + 128] = unfold(a, b).astype(BF16)

    wait_sent(oa.at[pl.ds(0, 7)], PH9A)
    wait_sent(ob.at[pl.ds(0, 7)], PH9B)
    @pl.when(odd == 0)
    def _():
        for k in range(7):
            wait_sent(m0, LASTZ + k)

    @pl.when(odd == 1)
    def _():
        for k in range(7):
            wait_sent(m0, LASTY + k)

    @pl.when(keeps)
    def _():
        wait_sent(s7.at[pl.ds(0, 7)], PH7)

    @pl.when(jnp.logical_not(keeps))
    def _():
        wait_sent(s7, PH7)


def body(tokens, lengths, norm_gain, w_in, log_step, eig_re, eig_im, in_mat, output_matrices, skip,
         w_glu, w_gate, state):
    args = (tokens, lengths.reshape(1, 32), norm_gain, w_in.swapaxes(1, 2), log_step, eig_re, eig_im,
            in_mat.swapaxes(3, 4), output_matrices, skip, w_glu, w_gate, state)
    return pl.pallas_call(
        kernel,
        name="decode",
        out_shape=(pltpu.VMEM((256, 512), BF16), pltpu.VMEM((2, 2, 32, 128), F32)),
        in_specs=[pl.BlockSpec(memory_space=pl.ANY)] * 13,
        out_specs=(pl.BlockSpec(memory_space=pltpu.VMEM),) * 2,
        scratch_shapes=[pltpu.VMEM(a.shape, a.dtype) for a in args]
        + [
            pltpu.VMEM((8, 16, 128), BF16),
            pltpu.VMEM((8, 16, 128), BF16),
            pltpu.VMEM((2, 8, 32, 128), BF16),
            pltpu.VMEM((2, 8, 8, 32, 128), BF16),
            pltpu.VMEM((8, 16, 128), BF16),
            pltpu.VMEM((8, 16, 128), BF16),
            pltpu.VMEM((8, 128, 128), BF16),
            pltpu.VMEM((8, 1, 128), F32),
            pltpu.VMEM((9, 16, 128), BF16),
            pltpu.VMEM((16, 128), BF16),
            pltpu.VMEM((2, 8, 128), BF16),
            pltpu.VMEM((2, 8, 8, 128), BF16),
            pltpu.VMEM((8, 32, 128), BF16),
            pltpu.VMEM((8, 32, 128), BF16),
            pltpu.VMEM((8, 16, 128), BF16),
            pltpu.VMEM((16, 128), BF16),
            pltpu.VMEM((8, 16, 128), BF16),
            pltpu.VMEM((8, 16, 128), BF16),
            pltpu.VMEM((8, 32, 128), BF16),
            pltpu.VMEM((8, 32, 128), BF16),
            pltpu.VMEM((8, 4, 16, 128), BF16),
            pltpu.VMEM((8, 4, 16, 128), BF16),
            pltpu.SemaphoreType.DMA((13,)),
            pltpu.SemaphoreType.DMA((COUNT,)),
            pltpu.SemaphoreType.DMA((COUNT,)),
        ],
        compiler_params=pltpu.CompilerParams(collective_id=0, has_side_effects=True),
    )(*args)


def solution(mesh):
    placed = (
        P(None, "dp"),
        P("dp"),
        P(None, "dp"),
        P(None, "dp", "tp"),
        P(None, "tp"),
        P(None, "tp", None),
        P(None, "tp", None),
        P(None, None, "tp", None, None),
        P(None, None, "tp", None, None),
        P(None, "tp"),
        P(None, "tp", "dp"),
        P(None, "tp", "dp"),
        P(None, None, "dp", "tp"),
    )
    return jax.shard_map(
        body,
        mesh=mesh,
        in_specs=placed,
        out_specs=(P(None, "dp"), P(None, None, "dp", "tp")),
        check_vma=False,
    )
```

time: 70 us -> 61 us (0.87)
  Pallas kernels: 64 us -> 58.8 us
  local copies, waits for them, and re-layouts: 4.87 us -> 1.33 us
    pallas_call x1, Pallas kernels: 64 us -> 58.8 us  [body(): pl.pallas_call(kernel, name='decode', out_shape=(pltpu.VMEM((256, 512), B...]
    unnamed x8 -> x2, local copies, waits for them, and re-layouts: 4.87 us -> 1.33 us
where the time goes in v2:
time: 61 us; the launch traced here: 60.8 us
  Pallas kernels  58.8 us (96%)
  local copies, waits for them, and re-layouts  1.33 us (2%)
  between operations  0.64 us (1%)
    pallas_call x1, Pallas kernels, body(): pl.pallas_call(kernel, name='decode', out_shape=(pltpu.VMEM((256, 512), B...  58.8 us
    unnamed x2, local copies, waits for them, and re-layouts  1.33 us

profile of v2, /device:TPU:1, one launch (start us, length us, event | category | flops | bytes accessed | tf_op | source)
XLA Modules:
  0.0 60.8 jit_solution(4365612578939342432)
XLA Ops:
  0.6 58.8 %decode.1 = (bf16[256,512]{1,0:T(8,128)(2,1)S(1)}, f32[2,2,32,128]{3,2,1,0:T(8,128)S(1)}) custom-call(bf16[256,512]{1,0:T(8,128)(2,1)} %tok_h.1, s32[1,32]{1,0:T(1,128)} %bitcast.5, f32[2,512]{1,0:T(2,128)} %gain_h.1, bf16[2,32,512]{2,1,0:T(8,128)(2,1)} %bitcast.3, f32[2,2]{1,0:T(2,128)} %ls_h.1, f32[2,2,64]{2,1,0:T(2,128)} %er_h.1, f32[2,2,64]{2,1,0:T(2,128)} %ei_h.1, ...), custom_call_target="tpu_custom_call" | custom-call | tf_op jit(solution)/shard_map/decode/pallas_call | solution.py:549
  59.5 0.7 %copy.17 = bf16[256,512]{1,0:T(8,128)(2,1)} copy(bf16[256,512]{1,0:T(8,128)(2,1)S(1)} %get-tuple-element.2) | data formatting | bytes 524288
  60.2 0.6 %copy.18 = f32[2,2,32,128]{3,2,1,0:T(8,128)} copy(f32[2,2,32,128]{3,2,1,0:T(8,128)S(1)} %get-tuple-element.3) | data formatting | bytes 131072

commit v3 on v0

v3 whole, which is shorter than its diff:
```python
import jax
import jax.numpy as jnp
from jax import lax
from jax.experimental import pallas as pl
from jax.experimental.pallas import tpu as pltpu
from jax.sharding import PartitionSpec as P

D = 4096
LEN_MAX = 4096
BLOCK_LEN = 256
NORM_EPS = 1e-06
MESH = pl.DeviceIdType.MESH
NT = (((1,), (1,)), ((), ()))
F32 = jnp.float32
BF16 = jnp.bfloat16

(PH1, RES0, PH2, ST1N, ST1S, STWN, STWS, PH3, PH4, RES1, PH5, PH6, PH7, PH9A, PH9B, GAIN, STATE, COUNTS, NEW) = range(19)
NEAR = 20
FARN = NEAR + 9
FARS = FARN + 8
LASTZ = FARS + 8
LASTY = LASTZ + 8
COUNT = LASTY + 8
NEAREST = (1, 7, 2, 6, 3, 5, 4)
FARTHEST = (4, 3, 5, 2, 6, 1, 7)


def roll(x, amount):
    amount = amount % 128
    return x if amount == 0 else pltpu.roll(x, amount, 1)


def groups4(rows):
    return lax.broadcasted_iota(jnp.int32, (rows, 128), 1) // 32


def low_half(rows):
    return lax.broadcasted_iota(jnp.int32, (rows, 128), 1) < 64


def pick4(parts, group):
    out = parts[3]
    for i in (2, 1, 0):
        out = jnp.where(group == i, parts[i], out)
    return out


def split2(x):
    hi = x.astype(BF16)
    lo = (x - hi.astype(F32)).astype(BF16)
    return hi, lo


def kernel(
    tok_h, len_h, gain_h, win_h, ls_h, er_h, ei_h, im_h, om_h, skip_h, glu_h, gate_h, st_h,
    mixed_ref, ns_ref,
    tok, lens, gain, win, ls, er, ei, im, om, skip, glu, gate, st,
    s1, r1, ws, w, wis, pk, wi, gb, rz, rz1, s2, r2, s3, r3, r4, m0, s5, r5, s7, r7, oa, ob,
    counts, st2, nsend, nrecv,
    lsem, ss, rs,
):
    tp = lax.axis_index("tp")
    d = lax.axis_index("dp")
    z = tp // 8
    y = lax.rem(tp, 8)
    x = d // 2
    core = lax.rem(d, 2)
    one = 2 * x + 1

    def at_y(k, dp=None):
        return {"tp": z * 8 + lax.rem(y + k, 8), "dp": one if dp is None else dp}

    def at_z(k, dp=None):
        return {"tp": lax.rem(z + k, 8) * 8 + y, "dp": one if dp is None else dp}

    def at_x(k, c=1):
        return {"tp": tp, "dp": 2 * lax.rem(x + k, 4) + c}

    def send(src, dst, sem, dev):
        pltpu.make_async_remote_copy(
            src_ref=src,
            dst_ref=dst,
            send_sem=ss.at[sem],
            recv_sem=rs.at[sem],
            device_id=dev,
            device_id_type=MESH,
        ).start()

    def wait_recv(ref, sem):
        with jax.named_scope(f"recv{sem}"):
            pltpu.make_async_copy(ref, ref, rs.at[sem]).wait()

    def wait_sent(ref, sem):
        pltpu.make_async_copy(ref, ref, ss.at[sem]).wait()

    def fold_low(t):
        n = t.shape[0] // 2
        return jnp.where(low_half(n), t[0:n], roll(t[n : 2 * n], 64))

    def fold_high(t):
        n = t.shape[0] // 2
        return jnp.where(low_half(n), roll(t[0:n], 64), t[n : 2 * n])

    def unfold(a, b):
        low = low_half(a.shape[0])
        return jnp.concatenate([jnp.where(low, a, roll(b, 64)), jnp.where(low, roll(a, 64), b)], axis=0)

    hbm = (tok_h, win_h, gain_h, glu_h, gate_h, len_h, st_h, ls_h, er_h, ei_h, im_h, om_h, skip_h)
    vmem = (tok, win, gain, glu, gate, lens, st, ls, er, ei, im, om, skip)
    loads = [pltpu.make_async_copy(a, b, lsem.at[i]) for i, (a, b) in enumerate(zip(hbm, vmem))]
    for copy in loads[:3]:
        copy.start()

    barrier = pltpu.get_barrier_semaphore()

    def greet(dev):
        pl.semaphore_signal(barrier, inc=1, device_id=dev, device_id_type=MESH)

    @pl.when(core == 1)
    def _():
        for k in FARTHEST:
            greet(at_y(k, 2 * x))
            greet(at_y(k))
            greet(at_z(k))
        for k in (2, 3, 1):
            greet(at_x(k, 0))
            greet(at_x(k))
        greet(at_x(0, 0))

    @pl.when(core == 0)
    def _():
        greet(at_x(0))

    for copy in loads[3:]:
        copy.start()
    group8 = groups4(8)

    def rows4(t):
        return pick4([jnp.broadcast_to(t[8 * i : 8 * i + 8], (8, 128)) for i in range(4)], group8)

    with jax.named_scope("load0"):
        for i in range(3):
            loads[i].wait()
    for xx in range(4):
        t = tok[64 * xx : 64 * xx + 64, :].astype(F32)
        scaled = (t * gain[0:1, :]).astype(BF16)
        part = lax.dot_general(scaled, win[0], NT, preferred_element_type=F32)
        sq = jnp.sum(t * t, axis=1, keepdims=True)
        packed = [
            jnp.concatenate([part[32 * h + 8 * i : 32 * h + 8 * i + 8, :] for i in range(4)], axis=1)
            for h in range(2)
        ]
        spread = [rows4(sq[32 * h : 32 * h + 32]) for h in range(2)]
        s1[xx] = jnp.concatenate(packed + spread, axis=0).astype(BF16)

    loads[3].wait()
    loads[4].wait()
    low32 = low_half(32)

    def pack_projection(layer):
        for q in range(4):
            g = glu[layer, :, 128 * q : 128 * q + 128].astype(F32)
            t = gate[layer, :, 128 * q : 128 * q + 128].astype(F32)
            ws[layer, 2 * q] = jnp.where(low32, g, roll(t, 64)).astype(BF16)
            ws[layer, 2 * q + 1] = jnp.where(low32, roll(g, 64), t).astype(BF16)

    pack_projection(0)

    half = lax.rem(y, 2)
    column = pl.ds(pl.multiple_of((y // 2) * 128, 128), 128)

    def pack_residual():
        for xx in range(4):
            t = tok[64 * xx : 64 * xx + 64, column].astype(F32)
            rz[xx] = fold_low(jnp.where(half == 1, roll(t, 64), t)).astype(BF16)

    def pack_input_weights():
        for q in range(4):
            t = win[1, :, 128 * q : 128 * q + 128].astype(F32)
            wis[2 * q] = fold_low(t).astype(BF16)
            wis[2 * q + 1] = fold_high(t).astype(BF16)

    def pack_gain():
        t = gain[1:2, column]
        return jnp.where(half == 1, roll(t, 64), t)[None]

    def assemble(g):
        for m in range(4):
            rows = pl.ds(pl.multiple_of((lax.rem(2 * m + g + 8 - 2 * x, 8) // 2) * 64, 64), 64)
            for q in range(4):
                a, b = (oa[2 * q, m], ob[2 * m, q]) if g == 0 else (ob[2 * m + 1, q], oa[2 * q + 1, m])
                mixed_ref[rows, 128 * q : 128 * q + 128] = unfold(a.astype(F32), b.astype(F32)).astype(BF16)

    @pl.when(core == 0)
    def _():
        with jax.named_scope("entry"):
            pl.semaphore_wait(barrier, 11)
        for k in (2, 3, 1, 0):
            send(s1.at[lax.rem(x + k, 4)], r1.at[d], PH1, at_x(k))
        for k in (0, *FARTHEST):
            send(ws.at[0, lax.rem(y + k, 8)], w.at[0, x, y, 0], FARS + k, at_y(k))
        loads[5].wait()
        counts[0] = (lens[...] // BLOCK_LEN).astype(F32)
        send(counts.at[0], counts.at[0], COUNTS, at_x(0))
        loads[6].wait()
        send(st, st2, STATE, at_x(0))

        @pl.when(d == z)
        def _():
            pack_residual()
            for k in range(4):
                send(rz.at[lax.rem(x + k, 4)], rz.at[4], RES0, at_x(k))

        pack_input_weights()
        for k in (0, *FARTHEST):
            send(wis.at[lax.rem(y + k, 8)], pk.at[0, y], STWS, at_y(k))
        gb[pl.ds(d, 1)] = pack_gain()
        for k in range(4):
            send(gb.at[d], gb.at[d], GAIN, at_x(k))
        pack_projection(1)
        for k in (0, *FARTHEST):
            send(ws.at[1, lax.rem(y + k, 8)], w.at[1, x, y, 0], ST1S, at_y(k))
        for i in range(7, 13):
            loads[i].wait()

        wait_sent(s1, PH1)
        for k in range(8):
            wait_sent(ws.at[0, 0], FARS + k)
        wait_sent(counts.at[0], COUNTS)
        wait_sent(st, STATE)

        @pl.when(d == z)
        def _():
            wait_sent(rz.at[pl.ds(0, 4)], RES0)

        wait_sent(wis, STWS)
        wait_sent(gb.at[pl.ds(0, 4)], GAIN)
        wait_sent(ws.at[1], ST1S)

        wait_recv(nrecv, NEW)
        ns_ref[...] = nrecv[...]
        wait_recv(oa.at[pl.ds(0, 4)], PH9A)
        wait_recv(ob.at[pl.ds(0, 4)], PH9B)
        assemble(0)

    @pl.when(core == 1)
    def _():
        r1[pl.ds(d, 1)] = s1[pl.ds(x, 1)]
        w[0, pl.ds(x, 1), pl.ds(y, 1), 1] = ws[0, pl.ds(y, 1)][None]

        @pl.when(d == z)
        def _():
            pack_residual()
            rz[4] = rz[pl.ds(x, 1)][0]

        with jax.named_scope("entry"):
            pl.semaphore_wait(barrier, 18)
        for k in (2, 3, 1):
            send(s1.at[lax.rem(x + k, 4)], r1.at[d], PH1, at_x(k))
        for k in FARTHEST:
            send(ws.at[0, lax.rem(y + k, 8)], w.at[0, x, y, 1], FARN + k, at_y(k))

        def pass_on(k):
            yy = lax.rem(y + 8 - k, 8)
            block = w.at[0, x, yy]
            if k:
                wait_recv(w.at[0, x, yy, 1], FARN + k)
            wait_recv(w.at[0, x, yy, 0], FARS + k)
            for r in (2, 3, 1):
                send(block, block, NEAR + r - 1, at_x(r))

        @pl.when(d == z)
        def _():
            for k in (2, 3, 1):
                send(rz.at[lax.rem(x + k, 4)], rz.at[4], RES0, at_x(k))

        loads[5].wait()
        counts[1] = (lens[...] // BLOCK_LEN).astype(F32)
        for i in range(6, 13):
            loads[i].wait()
        wait_recv(counts.at[0], COUNTS)
        wait_recv(st2, STATE)
        eye = lax.broadcasted_iota(jnp.int32, (32, 32), 0) == lax.broadcasted_iota(jnp.int32, (32, 32), 1)
        blocks = jnp.concatenate(
            [
                jnp.sum(jnp.where(eye, jnp.broadcast_to(counts[h], (32, 32)), 0.0), axis=1, keepdims=True)
                for h in range(2)
            ],
            axis=0,
        )
        factor = 2.0 / (1.0 + blocks * (4.0 * BLOCK_LEN / LEN_MAX))

        def by_group(slabs, sign):
            zero = jnp.zeros((16, 64), F32)
            cols = []
            for c in range(2):
                top = jnp.concatenate([slabs[2 * c], zero], axis=1)
                low = jnp.concatenate([zero, slabs[2 * c + 1]], axis=1)
                both = jnp.concatenate([top, low], axis=0)
                cols.append(both if c == 0 else sign * both)
            return jnp.concatenate([jnp.concatenate(cols, axis=1)] * 4, axis=0)

        def constants(layer):
            def row(ref):
                return jnp.concatenate([ref[layer, 0:1, :], ref[layer, 1:2, :]], axis=1)

            e_re, e_im = row(er), row(ei)
            rate = jnp.exp(ls[layer : layer + 1, :])
            rate = jnp.concatenate(
                [jnp.broadcast_to(rate[:, 0:1], (1, 64)), jnp.broadcast_to(rate[:, 1:2], (1, 64))], axis=1
            )
            step = rate * factor
            magnitude = jnp.exp(e_re * step)
            turned = e_im * step
            a_re = magnitude * jnp.cos(turned)
            a_im = magnitude * jnp.sin(turned)
            modulus = e_re * e_re + e_im * e_im
            b_re = ((a_re - 1.0) * e_re + a_im * e_im) / modulus
            b_im = (a_im * e_re - (a_re - 1.0) * e_im) / modulus
            u = jnp.concatenate([st2[layer, 0], st[layer, 0]], axis=0)
            v = jnp.concatenate([st2[layer, 1], st[layer, 1]], axis=0)
            k_re = a_re * u - a_im * v
            k_im = a_re * v + a_im * u
            hi, lo = split2(by_group([im[layer, c, g] for c in range(2) for g in range(2)], 1.0))
            in_cat = jnp.concatenate([hi, lo], axis=0)
            hi, lo = split2(by_group([om[layer, c, g] for c in range(2) for g in range(2)], -1.0))
            out_cat = jnp.concatenate([hi, lo, hi], axis=1)
            direct = jnp.concatenate([skip[layer : layer + 1, :]] * 4, axis=1)
            return k_re, k_im, b_re, b_im, in_cat, out_cat, direct

        def recurrence(layer, consts, total):
            k_re, k_im, b_re, b_im, in_cat, out_cat, direct = consts
            driven = (total[0:16] * lax.rsqrt(total[16:32] / D + NORM_EPS)).astype(BF16).astype(F32)
            spread = jnp.concatenate(
                [jnp.where(group8 == i, driven[8 * h : 8 * h + 8], 0.0) for h in range(2) for i in range(4)],
                axis=0,
            ).astype(BF16)
            drive = lax.dot_general(
                jnp.concatenate([spread, spread], axis=1), in_cat, (((1,), (0,)), ((), ())),
                preferred_element_type=F32,
            )
            d_re, d_im = drive[:, 0:128], drive[:, 128:256]
            n_re = k_re + b_re * d_re - b_im * d_im
            n_im = k_im + b_re * d_im + b_im * d_re
            for part, new in ((0, n_re), (1, n_im)):
                nsend[layer, part] = new[0:32]
                ns_ref[layer, part] = new[32:64]
            hi, lo = split2(jnp.concatenate([n_re, n_im], axis=1))
            full = lax.dot_general(
                jnp.concatenate([hi, hi, lo], axis=1), out_cat, NT, preferred_element_type=F32
            )
            value = jnp.concatenate([rows4(full[32 * h : 32 * h + 32]) for h in range(2)], axis=0)
            value = value + direct * driven
            inner = 0.7978845608028654 * (value + 0.044715 * (value * value * value))
            return (value * (0.5 * (1.0 + jnp.tanh(inner)))).astype(BF16)

        def gather_readout(layer, value, sem):
            s2[layer] = value
            r2[layer, pl.ds(y, 1)] = value[None]
            for k in FARTHEST:
                send(s2.at[layer], r2.at[layer, y], sem, at_y(k))

        def unpack_readout(layer):
            got = [r2[layer, j].astype(F32) for j in range(8)]
            tiles = []
            for h in range(2):
                for i in range(4):
                    cols = []
                    for q in range(2):
                        parts = [got[4 * q + j][8 * h : 8 * h + 8] for j in range(4)]
                        cols.append(pick4([roll(parts[j], 32 * (j - i)) for j in range(4)], group8))
                    tiles.append(jnp.concatenate(cols, axis=1))
            return jnp.concatenate(tiles, axis=0).astype(BF16)

        def project(layer, piece, k):
            return jnp.dot(
                piece, w[layer, k // 2, :, k % 2].reshape(256, 128), preferred_element_type=F32
            ).astype(BF16)

        def near(kind, block):
            for r in (2, 3, 1):
                send(block, block, NEAR + 3 * kind + r - 1, at_x(r))

        def wait_near(kind, ref):
            for r in range(1, 4):
                wait_recv(ref, NEAR + 3 * kind + r - 1)

        pass_on(0)
        consts0 = constants(0)
        for k in NEAREST[:4]:
            pass_on(k)
        wait_recv(r1.at[pl.ds(0, 7)], PH1)
        value = recurrence(0, consts0, jnp.sum(r1[...].astype(F32), axis=0))
        gather_readout(0, value, PH2)
        for k in NEAREST[4:]:
            pass_on(k)

        pack_input_weights()
        pk[1, pl.ds(y, 1)] = wis[pl.ds(y, 1)]
        for k in FARTHEST:
            send(wis.at[lax.rem(y + k, 8)], pk.at[1, y], STWN, at_y(k))
        gb[pl.ds(d, 1)] = pack_gain()
        for k in range(1, 4):
            send(gb.at[d], gb.at[d], GAIN, at_x(k))
        pack_projection(1)
        w[1, pl.ds(x, 1), pl.ds(y, 1), 1] = ws[1, pl.ds(y, 1)][None]
        for k in FARTHEST:
            send(ws.at[1, lax.rem(y + k, 8)], w.at[1, x, y, 1], ST1N, at_y(k))

        wait_recv(r2.at[0, pl.ds(0, 7)], PH2)
        piece = unpack_readout(0)
        wait_near(0, w.at[0, 0])
        for k in range(8):
            s3[k] = project(0, piece, k)
        for k in FARTHEST:
            send(s3.at[lax.rem(z + k, 8)], r3.at[z], PH3, at_z(k))
        r3[pl.ds(z, 1)] = s3[pl.ds(z, 1)]

        wait_recv(pk.at[1, pl.ds(0, 7)], STWN)
        wait_recv(pk.at[0], STWS)
        for h in range(2):
            for j in range(4):
                rows = unfold(pk[h, j].astype(F32), pk[h, 4 + j].astype(F32)).astype(BF16)
                wi[pl.ds(x, 1), h, 32 * j : 32 * j + 32, :] = rows[None]
        near(2, wi.at[x])
        wait_recv(w.at[1, 0, pl.ds(0, 7), 1], ST1N)
        wait_recv(w.at[1, 0, pl.ds(0, 8), 0], ST1S)
        near(1, w.at[1, x])
        send(nsend.at[0], nrecv.at[0], NEW, at_x(0, 0))

        @pl.when(d != z)
        def _():
            wait_recv(rz.at[4], RES0)

        def gated(parts, residual):
            linear, gate_sum = fold_low(parts), fold_high(parts)
            return (residual + linear * (1.0 / (1.0 + jnp.exp(-gate_sum)))).astype(BF16)

        residual0 = rz[4].astype(F32)
        wait_recv(r3.at[pl.ds(0, 7)], PH3)
        own = gated(jnp.sum(r3[...].astype(F32), axis=0), residual0)
        m0[...] = own
        r4[pl.ds(z, 1)] = own[None]
        for k in FARTHEST:
            send(m0, r4.at[z], PH4, at_z(k))

        alone = jnp.logical_and(x == 0, z < 2)

        @pl.when(jnp.logical_not(alone))
        def _():
            send(m0, rz1, RES1, {"tp": lax.rem(2 * x + z, 8) * 8 + y, "dp": (z // 2) * 2 + 1})

        @pl.when(alone)
        def _():
            rz1[...] = own

        consts1 = constants(1)
        wait_recv(gb.at[pl.ds(0, 7)], GAIN)
        low1 = low_half(1)
        gains = [jnp.where(low1, gb[2 * q], roll(gb[2 * q + 1], 64)) for q in range(4)]
        wait_near(2, wi.at[0])
        win_t = jnp.concatenate(
            [unfold(wi[q, 0].astype(F32), wi[q, 1].astype(F32)).astype(BF16) for q in range(4)], axis=1
        )

        wait_recv(r4.at[pl.ds(0, 7)], PH4)
        tiles = []
        sq = jnp.zeros((64, 1), F32)
        for q in range(4):
            cur = unfold(r4[2 * q].astype(F32), r4[2 * q + 1].astype(F32))
            sq = sq + jnp.sum(cur * cur, axis=1, keepdims=True)
            tiles.append((cur * gains[q]).astype(BF16))
        part = lax.dot_general(jnp.concatenate(tiles, axis=1), win_t, NT, preferred_element_type=F32)
        squares = [rows4(sq[32 * h : 32 * h + 32]) for h in range(2)]
        for q in range(2):
            for j in range(4):
                packed = []
                for h in range(2):
                    rows = [part[32 * h + 8 * i : 32 * h + 8 * i + 8, 128 * q : 128 * q + 128] for i in range(4)]
                    packed.append(pick4([roll(rows[i], 32 * (i - j)) for i in range(4)], group8))
                s5[4 * q + j] = jnp.concatenate(packed + squares, axis=0).astype(BF16)
        for k in FARTHEST:
            send(s5.at[lax.rem(y + k, 8)], r5.at[y], PH5, at_y(k))
        r5[pl.ds(y, 1)] = s5[pl.ds(y, 1)]
        wait_recv(r5.at[pl.ds(0, 7)], PH5)
        value = recurrence(1, consts1, jnp.sum(r5[...].astype(F32), axis=0))
        gather_readout(1, value, PH6)
        send(nsend.at[1], nrecv.at[1], NEW, at_x(0, 0))
        wait_near(1, w.at[1, 0])

        @pl.when(jnp.logical_not(alone))
        def _():
            wait_recv(rz1, RES1)

        wait_recv(r2.at[1, pl.ds(0, 7)], PH6)
        piece = unpack_readout(1)
        for k in range(8):
            s7[k] = project(1, piece, k)
        for k in (4, 5, 2, 3, 6, 7, 0, 1):
            to = lax.rem(2 * x + k, 8)
            zz = lax.rem(2 * x + to, 8)
            dev = {"tp": zz * 8 + y, "dp": (to // 2) * 2 + 1}
            if k > 1:
                send(s7.at[to], r7.at[z], PH7, dev)
            else:

                @pl.when(z != zz)
                def _(to=to, dev=dev):
                    send(s7.at[to], r7.at[z], PH7, dev)

                @pl.when(z == zz)
                def _(to=to):
                    r7[pl.ds(z, 1)] = s7[pl.ds(to, 1)]

        wait_sent(s1.at[pl.ds(0, 3)], PH1)
        for k in range(1, 8):
            wait_sent(ws.at[0, 0], FARN + k)
        for r in range(3):
            wait_sent(w.at[0, 0], NEAR + r)
            wait_sent(w.at[1, 0], NEAR + 3 + r)
            wait_sent(wi.at[0], NEAR + 6 + r)
        wait_sent(gb.at[pl.ds(0, 3)], GAIN)
        wait_sent(wis.at[pl.ds(0, 7)], STWN)
        wait_sent(ws.at[1, pl.ds(0, 7)], ST1N)
        wait_sent(r2.at[0, pl.ds(0, 7)], PH2)
        wait_sent(r2.at[1, pl.ds(0, 7)], PH6)
        wait_sent(s3.at[pl.ds(0, 7)], PH3)
        wait_sent(r4.at[pl.ds(0, 7)], PH4)
        wait_sent(s5.at[pl.ds(0, 7)], PH5)
        wait_sent(nsend, NEW)

        @pl.when(d == z)
        def _():
            wait_sent(rz.at[pl.ds(0, 3)], RES0)

        @pl.when(jnp.logical_not(alone))
        def _():
            wait_sent(m0, RES1)

        keeps = jnp.logical_or(z == lax.rem(4 * x, 8), z == lax.rem(4 * x + 1, 8))

        @pl.when(keeps)
        def _():
            wait_recv(r7.at[pl.ds(0, 7)], PH7)

        @pl.when(jnp.logical_not(keeps))
        def _():
            wait_recv(r7, PH7)

        own = gated(jnp.sum(r7[...].astype(F32), axis=0), rz1[...].astype(F32))

        odd = lax.rem(y + z, 2)
        core_a = 2 * x + lax.rem(y, 2)
        core_b = 2 * x + lax.rem(z, 2)

        def forward_a(zz):
            block = oa.at[y, zz // 2]
            for k in FARTHEST:
                send(block, block, PH9A, at_y(k, core_a))

            @pl.when(lax.rem(y, 2) == 0)
            def _():
                send(block, block, PH9A, at_x(0, 0))

        def forward_b(yy):
            block = ob.at[z, yy // 2]
            for k in FARTHEST:
                send(block, block, PH9B, at_z(k, core_b))

            @pl.when(lax.rem(z, 2) == 0)
            def _():
                send(block, block, PH9B, at_x(0, 0))

        def from_z(k):
            zz = lax.rem(z + 8 - k, 8)
            wait_recv(oa.at[y, zz // 2], LASTZ + k)
            forward_a(zz)

        def from_y(k):
            yy = lax.rem(y + 8 - k, 8)
            wait_recv(ob.at[z, yy // 2], LASTY + k)
            forward_b(yy)

        @pl.when(odd == 0)
        def _():
            oa[pl.ds(y, 1), pl.ds(z // 2, 1)] = own[None, None]
            for k in FARTHEST:
                send(oa.at[y, z // 2], oa.at[y, z // 2], LASTZ + k, at_z(k))
            forward_a(z)
            for k in NEAREST:
                (from_z if k % 2 == 0 else from_y)(k)

        @pl.when(odd == 1)
        def _():
            ob[pl.ds(z, 1), pl.ds(y // 2, 1)] = own[None, None]
            for k in FARTHEST:
                send(ob.at[z, y // 2], ob.at[z, y // 2], LASTY + k, at_y(k))
            forward_b(y)
            for k in NEAREST:
                (from_y if k % 2 == 0 else from_z)(k)

        def last_waits(buffer, sem, parity):
            @pl.when(parity == 0)
            def _():
                wait_recv(buffer.at[pl.ds(0, 4)], sem)

            @pl.when(parity == 1)
            def _():
                wait_recv(buffer.at[pl.ds(0, 3)], sem)

        last_waits(oa, PH9A, lax.rem(y, 2))
        last_waits(ob, PH9B, lax.rem(z, 2))
        assemble(1)

        def last_sent(buffer, sem, parity):
            @pl.when(parity == 0)
            def _():
                wait_sent(buffer, sem)

            @pl.when(parity == 1)
            def _():
                wait_sent(buffer.at[pl.ds(0, 7)], sem)

        last_sent(oa, PH9A, lax.rem(y, 2))
        last_sent(ob, PH9B, lax.rem(z, 2))

        @pl.when(odd == 0)
        def _():
            for k in FARTHEST:
                wait_sent(m0, LASTZ + k)

        @pl.when(odd == 1)
        def _():
            for k in FARTHEST:
                wait_sent(m0, LASTY + k)

        @pl.when(keeps)
        def _():
            wait_sent(s7.at[pl.ds(0, 7)], PH7)

        @pl.when(jnp.logical_not(keeps))
        def _():
            wait_sent(s7, PH7)


def body(tokens, lengths, norm_gain, w_in, log_step, eig_re, eig_im, in_mat, output_matrices, skip,
         w_glu, w_gate, state):
    args = (tokens, lengths.reshape(1, 32), norm_gain, w_in.swapaxes(1, 2), log_step, eig_re, eig_im,
            in_mat.swapaxes(3, 4), output_matrices, skip, w_glu, w_gate, state)
    return pl.pallas_call(
        kernel,
        name="decode",
        out_shape=(pltpu.VMEM((256, 512), BF16), pltpu.VMEM((2, 2, 32, 128), F32)),
        in_specs=[pl.BlockSpec(memory_space=pl.ANY)] * 13,
        out_specs=(pl.BlockSpec(memory_space=pltpu.VMEM),) * 2,
        scratch_shapes=[pltpu.VMEM(a.shape, a.dtype) for a in args]
        + [
            pltpu.VMEM((4, 32, 128), BF16),
            pltpu.VMEM((8, 32, 128), BF16),
            pltpu.VMEM((2, 8, 32, 128), BF16),
            pltpu.VMEM((2, 4, 8, 2, 32, 128), BF16),
            pltpu.VMEM((8, 16, 128), BF16),
            pltpu.VMEM((2, 8, 16, 128), BF16),
            pltpu.VMEM((4, 2, 128, 128), BF16),
            pltpu.VMEM((8, 1, 128), F32),
            pltpu.VMEM((5, 32, 128), BF16),
            pltpu.VMEM((32, 128), BF16),
            pltpu.VMEM((2, 16, 128), BF16),
            pltpu.VMEM((2, 8, 16, 128), BF16),
            pltpu.VMEM((8, 64, 128), BF16),
            pltpu.VMEM((8, 64, 128), BF16),
            pltpu.VMEM((8, 32, 128), BF16),
            pltpu.VMEM((32, 128), BF16),
            pltpu.VMEM((8, 32, 128), BF16),
            pltpu.VMEM((8, 32, 128), BF16),
            pltpu.VMEM((8, 64, 128), BF16),
            pltpu.VMEM((8, 64, 128), BF16),
            pltpu.VMEM((8, 4, 32, 128), BF16),
            pltpu.VMEM((8, 4, 32, 128), BF16),
            pltpu.VMEM((2, 1, 32), F32),
            pltpu.VMEM((2, 2, 32, 128), F32),
            pltpu.VMEM((2, 2, 32, 128), F32),
            pltpu.VMEM((2, 2, 32, 128), F32),
            pltpu.SemaphoreType.DMA((13,)),
            pltpu.SemaphoreType.DMA((COUNT,)),
            pltpu.SemaphoreType.DMA((COUNT,)),
        ],
        compiler_params=pltpu.CompilerParams(collective_id=0, has_side_effects=True),
    )(*args)


def solution(mesh):
    placed = (
        P(None, "dp"),
        P("dp"),
        P(None, "dp"),
        P(None, "dp", "tp"),
        P(None, "tp"),
        P(None, "tp", None),
        P(None, "tp", None),
        P(None, None, "tp", None, None),
        P(None, None, "tp", None, None),
        P(None, "tp"),
        P(None, "tp", "dp"),
        P(None, "tp", "dp"),
        P(None, None, "dp", "tp"),
    )
    return jax.shard_map(
        body,
        mesh=mesh,
        in_specs=placed,
        out_specs=(P(None, "dp"), P(None, None, "dp", "tp")),
        check_vma=False,
    )
```

time: 179 us -> 56.1 us (0.31); the launches traced: 177 us -> 56 us
  waiting for transfers between devices: 93.9 us -> 0 us
  starting transfers between devices: 57 us -> 0 us
  Pallas kernels: 0 us -> 54 us
  local copies, waits for them, and re-layouts: 17.9 us -> 1.33 us
  other arithmetic: 3.67 us -> 0 us
  matrix products: 3.06 us -> 0 us
    all_to_all x8 -> x0, waiting for transfers between devices: 93.9 us -> none  [the longest x4 61.2 us: sent_and_summed(): lax.all_to_all(pieces, axis, split_axis=0, concat_axis=0, tiled=True)]
    all_to_all x8 -> x0, starting transfers between devices: 57 us -> none  [the longest x4 33.5 us: sent_and_summed(): lax.all_to_all(pieces, axis, split_axis=0, concat_axis=0, tiled=True)]
    pallas_call x0 -> x1, Pallas kernels: none -> 54 us  [body(): pl.pallas_call(kernel, name='decode', out_shape=(pltpu.VMEM((256, 512), B...]
    unnamed x36 -> x2, local copies, waits for them, and re-layouts: 9.72 us -> 1.33 us
    transpose x2 -> x0, local copies, waits for them, and re-layouts: 3.18 us -> none  [split_up(): return jnp.moveaxis(array.reshape(*before, length, -1, *after), dim, 0)]
    dot_general x14 -> x0, matrix products: 3.06 us -> none  [the longest x2 0.61 us: body(): jnp.dot(scaled, w_in[layer_index], preferred_element_type=jnp.float32)]
  transfers between devices with their start and end apart: 8 -> 0, of which waited for: 8 -> 0; matrix products, arithmetic and copies ran while one was open for 1% -> 0% of each run, Pallas kernels for 0% -> 0%
where the time goes in v3:
time: 56.1 us; the launch traced here: 56 us
  Pallas kernels  54 us (96%)
  local copies, waits for them, and re-layouts  1.33 us (2%)
  between operations  0.64 us (1%)
    pallas_call x1, Pallas kernels, body(): pl.pallas_call(kernel, name='decode', out_shape=(pltpu.VMEM((256, 512), B...  54 us
    unnamed x2, local copies, waits for them, and re-layouts  1.33 us

profile of v3, /device:TPU:1, one launch (start us, length us, event | category | flops | bytes accessed | tf_op | source)
XLA Modules:
  0.0 56.0 jit_solution(5712573244414755906)
XLA Ops:
  0.6 54.0 %decode.1 = (bf16[256,512]{1,0:T(8,128)(2,1)S(1)}, f32[2,2,32,128]{3,2,1,0:T(8,128)S(1)}) custom-call(bf16[256,512]{1,0:T(8,128)(2,1)} %tok_h.1, s32[1,32]{1,0:T(1,128)} %bitcast.5, f32[2,512]{1,0:T(2,128)} %gain_h.1, bf16[2,32,512]{2,1,0:T(8,128)(2,1)} %bitcast.3, f32[2,2]{1,0:T(2,128)} %ls_h.1, f32[2,2,64]{2,1,0:T(2,128)} %er_h.1, f32[2,2,64]{2,1,0:T(2,128)} %ei_h.1, ...), custom_call_target="tpu_custom_call" | custom-call | tf_op jit(solution)/shard_map/decode/pallas_call | solution.py:650
  54.6 0.7 %copy.17 = bf16[256,512]{1,0:T(8,128)(2,1)} copy(bf16[256,512]{1,0:T(8,128)(2,1)S(1)} %get-tuple-element.2) | data formatting | bytes 524288
  55.3 0.6 %copy.18 = f32[2,2,32,128]{3,2,1,0:T(8,128)} copy(f32[2,2,32,128]{3,2,1,0:T(8,128)S(1)} %get-tuple-element.3) | data formatting | bytes 131072

commit v4 on v3

--- a/solution.py
+++ b/solution.py
@@ -14,14 +14,15 @@
 F32 = jnp.float32
 BF16 = jnp.bfloat16
 
-(PH1, RES0, PH2, ST1N, ST1S, STWN, STWS, PH3, PH4, RES1, PH5, PH6, PH7, PH9A, PH9B, GAIN, STATE, COUNTS, NEW) = range(19)
-NEAR = 20
-FARN = NEAR + 9
-FARS = FARN + 8
-LASTZ = FARS + 8
-LASTY = LASTZ + 8
-COUNT = LASTY + 8
-NEAREST = (1, 7, 2, 6, 3, 5, 4)
+(PH1, RES0, PH2, ST1, STW, PH3, PH4, RES1, PH5, PH6, PH7, PH9A, PH9B, GAIN, STATE, COUNTS, NEW, NEAR, NEAR1, NEARW) = range(20)
+FAR = 20
+LAST = FAR + 5
+RECV = LAST + 4
+BULK, SMALL, READ = range(3)
+SENT_ON = {NEAR: BULK, NEAR1: BULK, NEARW: BULK, NEW: BULK, STATE: READ, COUNTS: 3, PH3: SMALL, PH4: SMALL, PH5: SMALL,
+           PH2: READ, PH6: READ, STW: 4, PH1: 5, GAIN: 6, RES0: 7, RES1: 8, PH7: 9, PH9A: 10, PH9B: 10}
+SENT_LAST, SENT_A, SENT_B, SENT = 3, 11, 12, 13
+NEAREST = ((1, 7), (2, 6), (3, 5), (4,))
 FARTHEST = (4, 3, 5, 2, 6, 1, 7)
 
 
@@ -73,14 +74,22 @@
     def at_z(k, dp=None):
         return {"tp": lax.rem(z + k, 8) * 8 + y, "dp": one if dp is None else dp}
 
+    def far(k):
+        return FAR + min(k, 8 - k)
+
+    def last(k):
+        return LAST + min(k, 8 - k) - 1
+
     def at_x(k, c=1):
         return {"tp": tp, "dp": 2 * lax.rem(x + k, 4) + c}
 
-    def send(src, dst, sem, dev):
+    def send(src, dst, sem, dev, sent=None):
+        if sent is None:
+            sent = SENT_LAST if sem >= LAST else SMALL if sem >= FAR or sem == ST1 else SENT_ON[sem]
         pltpu.make_async_remote_copy(
             src_ref=src,
             dst_ref=dst,
-            send_sem=ss.at[sem],
+            send_sem=ss.at[sent],
             recv_sem=rs.at[sem],
             device_id=dev,
             device_id_type=MESH,
@@ -107,7 +116,13 @@
 
     hbm = (tok_h, win_h, gain_h, glu_h, gate_h, len_h, st_h, ls_h, er_h, ei_h, im_h, om_h, skip_h)
     vmem = (tok, win, gain, glu, gate, lens, st, ls, er, ei, im, om, skip)
-    loads = [pltpu.make_async_copy(a, b, lsem.at[i]) for i, (a, b) in enumerate(zip(hbm, vmem))]
+    group = (0, 0, 1, 2, 2, 3, 4, 5, 6, 7, 8, 9, 10)
+    loads = [pltpu.make_async_copy(a, b, lsem.at[i]) for i, a, b in zip(group, hbm, vmem)]
+
+    def wait_loaded(i):
+        ref = (w.at[0, pl.ds(0, 4), pl.ds(0, 5)], gain, w.at[0, 0], lens, st, ls, er, ei, im, om, skip)[i]
+        pltpu.make_async_copy(ref, ref, lsem.at[i]).wait()
+
     for copy in loads[:3]:
         copy.start()
 
@@ -139,8 +154,8 @@
         return pick4([jnp.broadcast_to(t[8 * i : 8 * i + 8], (8, 128)) for i in range(4)], group8)
 
     with jax.named_scope("load0"):
-        for i in range(3):
-            loads[i].wait()
+        wait_loaded(0)
+        wait_loaded(1)
     for xx in range(4):
         t = tok[64 * xx : 64 * xx + 64, :].astype(F32)
         scaled = (t * gain[0:1, :]).astype(BF16)
@@ -153,8 +168,7 @@
         spread = [rows4(sq[32 * h : 32 * h + 32]) for h in range(2)]
         s1[xx] = jnp.concatenate(packed + spread, axis=0).astype(BF16)
 
-    loads[3].wait()
-    loads[4].wait()
+    wait_loaded(2)
     low32 = low_half(32)
 
     def pack_projection(layer):
@@ -198,11 +212,11 @@
         for k in (2, 3, 1, 0):
             send(s1.at[lax.rem(x + k, 4)], r1.at[d], PH1, at_x(k))
         for k in (0, *FARTHEST):
-            send(ws.at[0, lax.rem(y + k, 8)], w.at[0, x, y, 0], FARS + k, at_y(k))
-        loads[5].wait()
+            send(ws.at[0, lax.rem(y + k, 8)], w.at[0, x, y, 0], far(k), at_y(k))
+        wait_loaded(3)
         counts[0] = (lens[...] // BLOCK_LEN).astype(F32)
         send(counts.at[0], counts.at[0], COUNTS, at_x(0))
-        loads[6].wait()
+        wait_loaded(4)
         send(st, st2, STATE, at_x(0))
 
         @pl.when(d == z)
@@ -213,29 +227,27 @@
 
         pack_input_weights()
         for k in (0, *FARTHEST):
-            send(wis.at[lax.rem(y + k, 8)], pk.at[0, y], STWS, at_y(k))
+            send(wis.at[lax.rem(y + k, 8)], pk.at[0, y], STW, at_y(k))
         gb[pl.ds(d, 1)] = pack_gain()
         for k in range(4):
             send(gb.at[d], gb.at[d], GAIN, at_x(k))
         pack_projection(1)
         for k in (0, *FARTHEST):
-            send(ws.at[1, lax.rem(y + k, 8)], w.at[1, x, y, 0], ST1S, at_y(k))
-        for i in range(7, 13):
-            loads[i].wait()
-
-        wait_sent(s1, PH1)
-        for k in range(8):
-            wait_sent(ws.at[0, 0], FARS + k)
-        wait_sent(counts.at[0], COUNTS)
-        wait_sent(st, STATE)
+            send(ws.at[1, lax.rem(y + k, 8)], w.at[1, x, y, 0], ST1, at_y(k))
+        for i in range(5, 11):
+            wait_loaded(i)
+
+        wait_sent(s1, SENT_ON[PH1])
+        wait_sent(w.at[0, 0], SMALL)
+        wait_sent(counts.at[0], SENT_ON[COUNTS])
+        wait_sent(st, READ)
 
         @pl.when(d == z)
         def _():
-            wait_sent(rz.at[pl.ds(0, 4)], RES0)
-
-        wait_sent(wis, STWS)
-        wait_sent(gb.at[pl.ds(0, 4)], GAIN)
-        wait_sent(ws.at[1], ST1S)
+            wait_sent(rz.at[pl.ds(0, 4)], SENT_ON[RES0])
+
+        wait_sent(wis, SENT_ON[STW])
+        wait_sent(gb.at[pl.ds(0, 4)], SENT_ON[GAIN])
 
         wait_recv(nrecv, NEW)
         ns_ref[...] = nrecv[...]
@@ -258,26 +270,27 @@
         for k in (2, 3, 1):
             send(s1.at[lax.rem(x + k, 4)], r1.at[d], PH1, at_x(k))
         for k in FARTHEST:
-            send(ws.at[0, lax.rem(y + k, 8)], w.at[0, x, y, 1], FARN + k, at_y(k))
-
-        def pass_on(k):
-            yy = lax.rem(y + 8 - k, 8)
-            block = w.at[0, x, yy]
-            if k:
-                wait_recv(w.at[0, x, yy, 1], FARN + k)
-            wait_recv(w.at[0, x, yy, 0], FARS + k)
-            for r in (2, 3, 1):
-                send(block, block, NEAR + r - 1, at_x(r))
+            send(ws.at[0, lax.rem(y + k, 8)], w.at[0, x, y, 1], far(k), at_y(k))
+
+        def pass_on(*distances):
+            if distances == (0,):
+                wait_recv(w.at[0, x, y, 0], FAR)
+            else:
+                wait_recv(w.at[0, 0, pl.ds(0, len(distances))], far(distances[0]))
+            for k in distances:
+                block = w.at[0, x, lax.rem(y + 8 - k, 8)]
+                for r in (2, 3, 1):
+                    send(block, block, NEAR, at_x(r))
 
         @pl.when(d == z)
         def _():
             for k in (2, 3, 1):
                 send(rz.at[lax.rem(x + k, 4)], rz.at[4], RES0, at_x(k))
 
-        loads[5].wait()
+        wait_loaded(3)
         counts[1] = (lens[...] // BLOCK_LEN).astype(F32)
-        for i in range(6, 13):
-            loads[i].wait()
+        for i in range(4, 11):
+            wait_loaded(i)
         wait_recv(counts.at[0], COUNTS)
         wait_recv(st2, STATE)
         eye = lax.broadcasted_iota(jnp.int32, (32, 32), 0) == lax.broadcasted_iota(jnp.int32, (32, 32), 1)
@@ -377,55 +390,49 @@
                 piece, w[layer, k // 2, :, k % 2].reshape(256, 128), preferred_element_type=F32
             ).astype(BF16)
 
-        def near(kind, block):
+        def near(sem, block):
             for r in (2, 3, 1):
-                send(block, block, NEAR + 3 * kind + r - 1, at_x(r))
-
-        def wait_near(kind, ref):
-            for r in range(1, 4):
-                wait_recv(ref, NEAR + 3 * kind + r - 1)
+                send(block, block, sem, at_x(r))
 
         pass_on(0)
         consts0 = constants(0)
-        for k in NEAREST[:4]:
-            pass_on(k)
+        for distances in NEAREST[:2]:
+            pass_on(*distances)
         wait_recv(r1.at[pl.ds(0, 7)], PH1)
         value = recurrence(0, consts0, jnp.sum(r1[...].astype(F32), axis=0))
         gather_readout(0, value, PH2)
-        for k in NEAREST[4:]:
-            pass_on(k)
+        for distances in NEAREST[2:]:
+            pass_on(*distances)
 
         pack_input_weights()
         pk[1, pl.ds(y, 1)] = wis[pl.ds(y, 1)]
         for k in FARTHEST:
-            send(wis.at[lax.rem(y + k, 8)], pk.at[1, y], STWN, at_y(k))
+            send(wis.at[lax.rem(y + k, 8)], pk.at[1, y], STW, at_y(k))
         gb[pl.ds(d, 1)] = pack_gain()
         for k in range(1, 4):
             send(gb.at[d], gb.at[d], GAIN, at_x(k))
         pack_projection(1)
         w[1, pl.ds(x, 1), pl.ds(y, 1), 1] = ws[1, pl.ds(y, 1)][None]
         for k in FARTHEST:
-            send(ws.at[1, lax.rem(y + k, 8)], w.at[1, x, y, 1], ST1N, at_y(k))
+            send(ws.at[1, lax.rem(y + k, 8)], w.at[1, x, y, 1], ST1, at_y(k))
 
         wait_recv(r2.at[0, pl.ds(0, 7)], PH2)
         piece = unpack_readout(0)
-        wait_near(0, w.at[0, 0])
+        wait_recv(w.at[0, pl.ds(0, 3)], NEAR)
         for k in range(8):
             s3[k] = project(0, piece, k)
         for k in FARTHEST:
             send(s3.at[lax.rem(z + k, 8)], r3.at[z], PH3, at_z(k))
         r3[pl.ds(z, 1)] = s3[pl.ds(z, 1)]
 
-        wait_recv(pk.at[1, pl.ds(0, 7)], STWN)
-        wait_recv(pk.at[0], STWS)
+        wait_recv(w.at[0, pl.ds(0, 3), pl.ds(0, 5), 0, pl.ds(0, 16)], STW)
         for h in range(2):
             for j in range(4):
                 rows = unfold(pk[h, j].astype(F32), pk[h, 4 + j].astype(F32)).astype(BF16)
                 wi[pl.ds(x, 1), h, 32 * j : 32 * j + 32, :] = rows[None]
-        near(2, wi.at[x])
-        wait_recv(w.at[1, 0, pl.ds(0, 7), 1], ST1N)
-        wait_recv(w.at[1, 0, pl.ds(0, 8), 0], ST1S)
-        near(1, w.at[1, x])
+        near(NEARW, wi.at[x])
+        wait_recv(w.at[0, pl.ds(0, 3), pl.ds(0, 5), 0], ST1)
+        near(NEAR1, w.at[1, x])
         send(nsend.at[0], nrecv.at[0], NEW, at_x(0, 0))
 
         @pl.when(d != z)
@@ -458,7 +465,7 @@
         wait_recv(gb.at[pl.ds(0, 7)], GAIN)
         low1 = low_half(1)
         gains = [jnp.where(low1, gb[2 * q], roll(gb[2 * q + 1], 64)) for q in range(4)]
-        wait_near(2, wi.at[0])
+        wait_recv(wi.at[pl.ds(0, 3)], NEARW)
         win_t = jnp.concatenate(
             [unfold(wi[q, 0].astype(F32), wi[q, 1].astype(F32)).astype(BF16) for q in range(4)], axis=1
         )
@@ -486,7 +493,7 @@
         value = recurrence(1, consts1, jnp.sum(r5[...].astype(F32), axis=0))
         gather_readout(1, value, PH6)
         send(nsend.at[1], nrecv.at[1], NEW, at_x(0, 0))
-        wait_near(1, w.at[1, 0])
+        wait_recv(w.at[1, pl.ds(0, 3)], NEAR1)
 
         @pl.when(jnp.logical_not(alone))
         def _():
@@ -512,30 +519,20 @@
                 def _(to=to):
                     r7[pl.ds(z, 1)] = s7[pl.ds(to, 1)]
 
-        wait_sent(s1.at[pl.ds(0, 3)], PH1)
-        for k in range(1, 8):
-            wait_sent(ws.at[0, 0], FARN + k)
-        for r in range(3):
-            wait_sent(w.at[0, 0], NEAR + r)
-            wait_sent(w.at[1, 0], NEAR + 3 + r)
-            wait_sent(wi.at[0], NEAR + 6 + r)
-        wait_sent(gb.at[pl.ds(0, 3)], GAIN)
-        wait_sent(wis.at[pl.ds(0, 7)], STWN)
-        wait_sent(ws.at[1, pl.ds(0, 7)], ST1N)
-        wait_sent(r2.at[0, pl.ds(0, 7)], PH2)
-        wait_sent(r2.at[1, pl.ds(0, 7)], PH6)
-        wait_sent(s3.at[pl.ds(0, 7)], PH3)
-        wait_sent(r4.at[pl.ds(0, 7)], PH4)
-        wait_sent(s5.at[pl.ds(0, 7)], PH5)
-        wait_sent(nsend, NEW)
+        wait_sent(s1.at[pl.ds(0, 3)], SENT_ON[PH1])
+        wait_sent(w, BULK)
+        wait_sent(w.at[0, pl.ds(0, 3), pl.ds(0, 7)], SMALL)
+        wait_sent(r4.at[pl.ds(0, 7)], READ)
+        wait_sent(gb.at[pl.ds(0, 3)], SENT_ON[GAIN])
+        wait_sent(wis.at[pl.ds(0, 7)], SENT_ON[STW])
 
         @pl.when(d == z)
         def _():
-            wait_sent(rz.at[pl.ds(0, 3)], RES0)
+            wait_sent(rz.at[pl.ds(0, 3)], SENT_ON[RES0])
 
         @pl.when(jnp.logical_not(alone))
         def _():
-            wait_sent(m0, RES1)
+            wait_sent(m0, SENT_ON[RES1])
 
         keeps = jnp.logical_or(z == lax.rem(4 * x, 8), z == lax.rem(4 * x + 1, 8))
 
@@ -560,7 +557,7 @@
 
             @pl.when(lax.rem(y, 2) == 0)
             def _():
-                send(block, block, PH9A, at_x(0, 0))
+                send(block, block, PH9A, at_x(0, 0), SENT_A)
 
         def forward_b(yy):
             block = ob.at[z, yy // 2]
@@ -569,35 +566,37 @@
 
             @pl.when(lax.rem(z, 2) == 0)
             def _():
-                send(block, block, PH9B, at_x(0, 0))
-
-        def from_z(k):
-            zz = lax.rem(z + 8 - k, 8)
-            wait_recv(oa.at[y, zz // 2], LASTZ + k)
-            forward_a(zz)
-
-        def from_y(k):
-            yy = lax.rem(y + 8 - k, 8)
-            wait_recv(ob.at[z, yy // 2], LASTY + k)
-            forward_b(yy)
+                send(block, block, PH9B, at_x(0, 0), SENT_B)
+
+        def from_z(distances):
+            wait_recv(r4.at[pl.ds(0, len(distances))], last(distances[0]))
+            for k in distances:
+                forward_a(lax.rem(z + 8 - k, 8))
+
+        def from_y(distances):
+            wait_recv(r4.at[pl.ds(0, len(distances))], last(distances[0]))
+            for k in distances:
+                forward_b(lax.rem(y + 8 - k, 8))
 
         @pl.when(odd == 0)
         def _():
+            block = oa.at[y, z // 2]
             oa[pl.ds(y, 1), pl.ds(z // 2, 1)] = own[None, None]
             for k in FARTHEST:
-                send(oa.at[y, z // 2], oa.at[y, z // 2], LASTZ + k, at_z(k))
+                send(block, block, last(k), at_z(k))
             forward_a(z)
-            for k in NEAREST:
-                (from_z if k % 2 == 0 else from_y)(k)
+            for distances in NEAREST:
+                (from_z if distances[0] % 2 == 0 else from_y)(distances)
 
         @pl.when(odd == 1)
         def _():
+            block = ob.at[z, y // 2]
             ob[pl.ds(z, 1), pl.ds(y // 2, 1)] = own[None, None]
             for k in FARTHEST:
-                send(ob.at[z, y // 2], ob.at[z, y // 2], LASTY + k, at_y(k))
+                send(block, block, last(k), at_y(k))
             forward_b(y)
-            for k in NEAREST:
-                (from_y if k % 2 == 0 else from_z)(k)
+            for distances in NEAREST:
+                (from_y if distances[0] % 2 == 0 else from_z)(distances)
 
         def last_waits(buffer, sem, parity):
             @pl.when(parity == 0)
@@ -610,44 +609,47 @@
 
         last_waits(oa, PH9A, lax.rem(y, 2))
         last_waits(ob, PH9B, lax.rem(z, 2))
-        assemble(1)
-
-        def last_sent(buffer, sem, parity):
-            @pl.when(parity == 0)
+        with jax.named_scope("assemble"):
+            assemble(1)
+
+        with jax.named_scope("sent"):
+            wait_sent(w.at[0, pl.ds(0, 4), pl.ds(0, 7)], SENT_ON[PH9A])
+
+            @pl.when(lax.rem(y, 2) == 0)
             def _():
-                wait_sent(buffer, sem)
-
-            @pl.when(parity == 1)
+                wait_sent(oa.at[0], SENT_A)
+
+            @pl.when(lax.rem(z, 2) == 0)
             def _():
-                wait_sent(buffer.at[pl.ds(0, 7)], sem)
-
-        last_sent(oa, PH9A, lax.rem(y, 2))
-        last_sent(ob, PH9B, lax.rem(z, 2))
-
-        @pl.when(odd == 0)
-        def _():
-            for k in FARTHEST:
-                wait_sent(m0, LASTZ + k)
-
-        @pl.when(odd == 1)
-        def _():
-            for k in FARTHEST:
-                wait_sent(m0, LASTY + k)
+                wait_sent(ob.at[0], SENT_B)
+
+        wait_sent(r4.at[pl.ds(0, 7)], SENT_LAST)
 
         @pl.when(keeps)
         def _():
-            wait_sent(s7.at[pl.ds(0, 7)], PH7)
+            wait_sent(s7.at[pl.ds(0, 7)], SENT_ON[PH7])
 
         @pl.when(jnp.logical_not(keeps))
         def _():
-            wait_sent(s7, PH7)
+            wait_sent(s7, SENT_ON[PH7])
+
+
+def hand_over(mixed, state, mixed_h, state_h, sems):
+    copies = [
+        pltpu.make_async_copy(mixed, mixed_h, sems.at[0]),
+        pltpu.make_async_copy(state, state_h, sems.at[1]),
+    ]
+    for copy in copies:
+        copy.start()
+    for copy in copies:
+        copy.wait()
 
 
 def body(tokens, lengths, norm_gain, w_in, log_step, eig_re, eig_im, in_mat, output_matrices, skip,
          w_glu, w_gate, state):
     args = (tokens, lengths.reshape(1, 32), norm_gain, w_in.swapaxes(1, 2), log_step, eig_re, eig_im,
             in_mat.swapaxes(3, 4), output_matrices, skip, w_glu, w_gate, state)
-    return pl.pallas_call(
+    mixed, new_state = pl.pallas_call(
         kernel,
         name="decode",
         out_shape=(pltpu.VMEM((256, 512), BF16), pltpu.VMEM((2, 2, 32, 128), F32)),
@@ -681,12 +683,21 @@
             pltpu.VMEM((2, 2, 32, 128), F32),
             pltpu.VMEM((2, 2, 32, 128), F32),
             pltpu.VMEM((2, 2, 32, 128), F32),
-            pltpu.SemaphoreType.DMA((13,)),
-            pltpu.SemaphoreType.DMA((COUNT,)),
-            pltpu.SemaphoreType.DMA((COUNT,)),
+            pltpu.SemaphoreType.DMA((11,)),
+            pltpu.SemaphoreType.DMA((SENT,)),
+            pltpu.SemaphoreType.DMA((RECV,)),
         ],
         compiler_params=pltpu.CompilerParams(collective_id=0, has_side_effects=True),
     )(*args)
+    inside = [pltpu.with_memory_space_constraint(a, pltpu.VMEM) for a in (mixed, new_state)]
+    return pl.pallas_call(
+        hand_over,
+        name="hand_over",
+        out_shape=(jax.ShapeDtypeStruct((256, 512), BF16), jax.ShapeDtypeStruct((2, 2, 32, 128), F32)),
+        in_specs=[pl.BlockSpec(memory_space=pltpu.VMEM)] * 2,
+        out_specs=(pl.BlockSpec(memory_space=pl.ANY),) * 2,
+        scratch_shapes=[pltpu.SemaphoreType.DMA((2,))],
+    )(*inside)
 
 
 def solution(mesh):

time: 56.1 us -> 54.9 us (0.979)
  local copies, waits for them, and re-layouts: 1.33 us -> 0 us
    unnamed x2 -> x0, local copies, waits for them, and re-layouts: 1.33 us -> none
    pallas_call x0 -> x1, Pallas kernels: none -> 0.74 us  [body(): pl.pallas_call(hand_over, name='hand_over', out_shape=(jax.ShapeDtypeStru...]
where the time goes in v4:
time: 54.9 us; the launch traced here: 54.8 us
  Pallas kernels  54.2 us (99%)
  between operations  0.64 us (1%)
    pallas_call x1, Pallas kernels, body(): pl.pallas_call(kernel, name='decode', out_shape=(pltpu.VMEM((256, 512), B...  53.4 us

profile of v4, /device:TPU:1, one launch (start us, length us, event | category | flops | bytes accessed | tf_op | source)
XLA Modules:
  0.0 54.8 jit_solution(12732902857420441985)
XLA Ops:
  0.6 53.4 %decode.1 = (bf16[256,512]{1,0:T(8,128)(2,1)S(1)}, f32[2,2,32,128]{3,2,1,0:T(8,128)S(1)}) custom-call(bf16[256,512]{1,0:T(8,128)(2,1)} %tok_h.1, s32[1,32]{1,0:T(1,128)} %bitcast.5, f32[2,512]{1,0:T(2,128)} %gain_h.1, bf16[2,32,512]{2,1,0:T(8,128)(2,1)} %bitcast.3, f32[2,2]{1,0:T(2,128)} %ls_h.1, f32[2,2,64]{2,1,0:T(2,128)} %er_h.1, f32[2,2,64]{2,1,0:T(2,128)} %ei_h.1, ...), custom_call_target="tpu_custom_call" | custom-call | tf_op jit(solution)/shard_map/decode/pallas_call | solution.py:652
  54.1 0.7 %hand_over.1 = (bf16[256,512]{1,0:T(8,128)(2,1)}, f32[2,2,32,128]{3,2,1,0:T(8,128)}) custom-call(bf16[256,512]{1,0:T(8,128)(2,1)S(1)} %get-tuple-element.4.mixed, f32[2,2,32,128]{3,2,1,0:T(8,128)S(1)} %get-tuple-element.5.state), custom_call_target="tpu_custom_call" | custom-call | tf_op jit(solution)/shard_map/hand_over/pallas_call | solution.py:693

commit v5 on v4

--- a/solution.py
+++ b/solution.py
@@ -134,8 +134,9 @@
     @pl.when(core == 1)
     def _():
         for k in FARTHEST:
+            greet(at_y(k))
             greet(at_y(k, 2 * x))
-            greet(at_y(k))
+        for k in FARTHEST:
             greet(at_z(k))
         for k in (2, 3, 1):
             greet(at_x(k, 0))
@@ -336,8 +337,8 @@
             k_im = a_re * v + a_im * u
             hi, lo = split2(by_group([im[layer, c, g] for c in range(2) for g in range(2)], 1.0))
             in_cat = jnp.concatenate([hi, lo], axis=0)
-            hi, lo = split2(by_group([om[layer, c, g] for c in range(2) for g in range(2)], -1.0))
-            out_cat = jnp.concatenate([hi, lo, hi], axis=1)
+            hi, lo = split2(by_group([om[layer, c, g] for c in range(2) for g in range(2)], -1.0).T)
+            out_cat = jnp.concatenate([hi, lo, hi], axis=0)
             direct = jnp.concatenate([skip[layer : layer + 1, :]] * 4, axis=1)
             return k_re, k_im, b_re, b_im, in_cat, out_cat, direct
 
@@ -360,7 +361,8 @@
                 ns_ref[layer, part] = new[32:64]
             hi, lo = split2(jnp.concatenate([n_re, n_im], axis=1))
             full = lax.dot_general(
-                jnp.concatenate([hi, hi, lo], axis=1), out_cat, NT, preferred_element_type=F32
+                jnp.concatenate([hi, hi, lo], axis=1), out_cat, (((1,), (0,)), ((), ())),
+                preferred_element_type=F32,
             )
             value = jnp.concatenate([rows4(full[32 * h : 32 * h + 32]) for h in range(2)], axis=0)
             value = value + direct * driven
@@ -385,10 +387,11 @@
                     tiles.append(jnp.concatenate(cols, axis=1))
             return jnp.concatenate(tiles, axis=0).astype(BF16)
 
-        def project(layer, piece, k):
-            return jnp.dot(
-                piece, w[layer, k // 2, :, k % 2].reshape(256, 128), preferred_element_type=F32
-            ).astype(BF16)
+        def project(layer, piece, xx, out):
+            rhs = jnp.concatenate([w[layer, xx, :, h].reshape(256, 128) for h in range(2)], axis=1)
+            both = jnp.dot(piece, rhs, preferred_element_type=F32).astype(BF16)
+            out[2 * xx] = both[:, 0:128]
+            out[2 * xx + 1] = both[:, 128:256]
 
         def near(sem, block):
             for r in (2, 3, 1):
@@ -419,8 +422,8 @@
         wait_recv(r2.at[0, pl.ds(0, 7)], PH2)
         piece = unpack_readout(0)
         wait_recv(w.at[0, pl.ds(0, 3)], NEAR)
-        for k in range(8):
-            s3[k] = project(0, piece, k)
+        for xx in range(4):
+            project(0, piece, xx, s3)
         for k in FARTHEST:
             send(s3.at[lax.rem(z + k, 8)], r3.at[z], PH3, at_z(k))
         r3[pl.ds(z, 1)] = s3[pl.ds(z, 1)]
@@ -467,7 +470,7 @@
         gains = [jnp.where(low1, gb[2 * q], roll(gb[2 * q + 1], 64)) for q in range(4)]
         wait_recv(wi.at[pl.ds(0, 3)], NEARW)
         win_t = jnp.concatenate(
-            [unfold(wi[q, 0].astype(F32), wi[q, 1].astype(F32)).astype(BF16) for q in range(4)], axis=1
+            [unfold(wi[q, 0].astype(F32), wi[q, 1].astype(F32)).T.astype(BF16) for q in range(4)], axis=0
         )
 
         wait_recv(r4.at[pl.ds(0, 7)], PH4)
@@ -477,7 +480,7 @@
             cur = unfold(r4[2 * q].astype(F32), r4[2 * q + 1].astype(F32))
             sq = sq + jnp.sum(cur * cur, axis=1, keepdims=True)
             tiles.append((cur * gains[q]).astype(BF16))
-        part = lax.dot_general(jnp.concatenate(tiles, axis=1), win_t, NT, preferred_element_type=F32)
+        part = jnp.dot(jnp.concatenate(tiles, axis=1), win_t, preferred_element_type=F32)
         squares = [rows4(sq[32 * h : 32 * h + 32]) for h in range(2)]
         for q in range(2):
             for j in range(4):
@@ -501,8 +504,8 @@
 
         wait_recv(r2.at[1, pl.ds(0, 7)], PH6)
         piece = unpack_readout(1)
-        for k in range(8):
-            s7[k] = project(1, piece, k)
+        for xx in range(4):
+            project(1, piece, xx, s7)
         for k in (4, 5, 2, 3, 6, 7, 0, 1):
             to = lax.rem(2 * x + k, 8)
             zz = lax.rem(2 * x + to, 8)
@@ -550,10 +553,20 @@
         core_a = 2 * x + lax.rem(y, 2)
         core_b = 2 * x + lax.rem(z, 2)
 
+        def others(mine, serve):
+            for t in (0, 1, 2, 7, 3, 6, 5, 4):
+
+                @pl.when(mine != t)
+                def _(t=t):
+                    serve(t)
+
+        def apart(a, b):
+            k = lax.rem(a + 8 - b, 8)
+            return jnp.minimum(k, 8 - k)
+
         def forward_a(zz):
             block = oa.at[y, zz // 2]
-            for k in FARTHEST:
-                send(block, block, PH9A, at_y(k, core_a))
+            others(y, lambda t: send(block, block, PH9A, {"tp": z * 8 + t, "dp": core_a}))
 
             @pl.when(lax.rem(y, 2) == 0)
             def _():
@@ -561,8 +574,7 @@
 
         def forward_b(yy):
             block = ob.at[z, yy // 2]
-            for k in FARTHEST:
-                send(block, block, PH9B, at_z(k, core_b))
+            others(z, lambda t: send(block, block, PH9B, {"tp": t * 8 + y, "dp": core_b}))
 
             @pl.when(lax.rem(z, 2) == 0)
             def _():
@@ -582,8 +594,7 @@
         def _():
             block = oa.at[y, z // 2]
             oa[pl.ds(y, 1), pl.ds(z // 2, 1)] = own[None, None]
-            for k in FARTHEST:
-                send(block, block, last(k), at_z(k))
+            others(z, lambda t: send(block, block, LAST + apart(t, z) - 1, {"tp": t * 8 + y, "dp": one}, SENT_LAST))
             forward_a(z)
             for distances in NEAREST:
                 (from_z if distances[0] % 2 == 0 else from_y)(distances)
@@ -592,8 +603,7 @@
         def _():
             block = ob.at[z, y // 2]
             ob[pl.ds(z, 1), pl.ds(y // 2, 1)] = own[None, None]
-            for k in FARTHEST:
-                send(block, block, last(k), at_y(k))
+            others(y, lambda t: send(block, block, LAST + apart(t, y) - 1, {"tp": z * 8 + t, "dp": one}, SENT_LAST))
             forward_b(y)
             for distances in NEAREST:
                 (from_y if distances[0] % 2 == 0 else from_z)(distances)

time: 54.9 us -> 54.3 us (0.989)
  Pallas kernels: 54.2 us -> 53.5 us
    pallas_call x1, Pallas kernels: 53.4 us -> 52.8 us  [body(): pl.pallas_call(kernel, name='decode', out_shape=(pltpu.VMEM((256, 512), B...]
where the time goes in v5:
time: 54.3 us; the launch traced here: 54.1 us
  Pallas kernels  53.5 us (99%)
  between operations  0.64 us (1%)
    pallas_call x1, Pallas kernels, body(): pl.pallas_call(kernel, name='decode', out_shape=(pltpu.VMEM((256, 512), B...  52.8 us

profile of v5, /device:TPU:1, one launch (start us, length us, event | category | flops | bytes accessed | tf_op | source)
XLA Modules:
  0.0 54.1 jit_solution(285034918436911861)
XLA Ops:
  0.6 52.8 %decode.1 = (bf16[256,512]{1,0:T(8,128)(2,1)S(1)}, f32[2,2,32,128]{3,2,1,0:T(8,128)S(1)}) custom-call(bf16[256,512]{1,0:T(8,128)(2,1)} %tok_h.1, s32[1,32]{1,0:T(1,128)} %bitcast.5, f32[2,512]{1,0:T(2,128)} %gain_h.1, bf16[2,32,512]{2,1,0:T(8,128)(2,1)} %bitcast.3, f32[2,2]{1,0:T(2,128)} %ls_h.1, f32[2,2,64]{2,1,0:T(2,128)} %er_h.1, f32[2,2,64]{2,1,0:T(2,128)} %ei_h.1, ...), custom_call_target="tpu_custom_call" | custom-call | tf_op jit(solution)/shard_map/decode/pallas_call | solution.py:662
  53.4 0.7 %hand_over.1 = (bf16[256,512]{1,0:T(8,128)(2,1)}, f32[2,2,32,128]{3,2,1,0:T(8,128)}) custom-call(bf16[256,512]{1,0:T(8,128)(2,1)S(1)} %get-tuple-element.4.mixed, f32[2,2,32,128]{3,2,1,0:T(8,128)S(1)} %get-tuple-element.5.state), custom_call_target="tpu_custom_call" | custom-call | tf_op jit(solution)/shard_map/hand_over/pallas_call | solution.py:703

commit v6 on v5

--- a/solution.py
+++ b/solution.py
@@ -21,7 +21,7 @@
 BULK, SMALL, READ = range(3)
 SENT_ON = {NEAR: BULK, NEAR1: BULK, NEARW: BULK, NEW: BULK, STATE: READ, COUNTS: 3, PH3: SMALL, PH4: SMALL, PH5: SMALL,
            PH2: READ, PH6: READ, STW: 4, PH1: 5, GAIN: 6, RES0: 7, RES1: 8, PH7: 9, PH9A: 10, PH9B: 10}
-SENT_LAST, SENT_A, SENT_B, SENT = 3, 11, 12, 13
+SENT_LAST, SENT_A, SENT_B, RELAY_A, RELAY_B, LOW, SENT = 3, 11, 12, 13, 14, 15, 17
 NEAREST = ((1, 7), (2, 6), (3, 5), (4,))
 FARTHEST = (4, 3, 5, 2, 6, 1, 7)
 
@@ -553,29 +553,32 @@
         core_a = 2 * x + lax.rem(y, 2)
         core_b = 2 * x + lax.rem(z, 2)
 
-        def others(mine, serve):
-            for t in (0, 1, 2, 7, 3, 6, 5, 4):
-
-                @pl.when(mine != t)
-                def _(t=t):
-                    serve(t)
+        ORDER = (0, 1, 2, 7, 3, 6, 5, 4)
+
+        def others(mine, serve, first=0):
+            for t in ORDER:
+                if t >= first:
+
+                    @pl.when(mine != t)
+                    def _(t=t):
+                        serve(t)
 
         def apart(a, b):
             k = lax.rem(a + 8 - b, 8)
             return jnp.minimum(k, 8 - k)
 
-        def forward_a(zz):
-            block = oa.at[y, zz // 2]
-            others(y, lambda t: send(block, block, PH9A, {"tp": z * 8 + t, "dp": core_a}))
-
+        def across(block, sent):
+            others(y, lambda t: send(block, block, PH9A, {"tp": z * 8 + t, "dp": core_a}, sent))
+
+        def along(block, sent, first=0):
+            others(z, lambda t: send(block, block, PH9B, {"tp": t * 8 + y, "dp": core_b}, sent), first)
+
+        def to_own_a(block):
             @pl.when(lax.rem(y, 2) == 0)
             def _():
                 send(block, block, PH9A, at_x(0, 0), SENT_A)
 
-        def forward_b(yy):
-            block = ob.at[z, yy // 2]
-            others(z, lambda t: send(block, block, PH9B, {"tp": t * 8 + y, "dp": core_b}))
-
+        def to_own_b(block):
             @pl.when(lax.rem(z, 2) == 0)
             def _():
                 send(block, block, PH9B, at_x(0, 0), SENT_B)
@@ -583,19 +586,41 @@
         def from_z(distances):
             wait_recv(r4.at[pl.ds(0, len(distances))], last(distances[0]))
             for k in distances:
-                forward_a(lax.rem(z + 8 - k, 8))
+                block = oa.at[y, lax.rem(z + 8 - k, 8) // 2]
+                if distances[0] < 3:
+                    across(block, RELAY_A)
+                else:
+
+                    @pl.when(z > 1)
+                    def _(block=block):
+                        across(block, RELAY_A)
+
+                to_own_a(block)
 
         def from_y(distances):
             wait_recv(r4.at[pl.ds(0, len(distances))], last(distances[0]))
             for k in distances:
-                forward_b(lax.rem(y + 8 - k, 8))
+                block = ob.at[z, lax.rem(y + 8 - k, 8) // 2]
+                along(block, RELAY_B, 2)
+                to_own_b(block)
+
+        def straight(t, block, sem, parity):
+            for k in FARTHEST:
+                send(block, block, sem, {"tp": t * 8 + lax.rem(y + k, 8), "dp": 2 * x + parity}, LOW + t)
 
         @pl.when(odd == 0)
         def _():
             block = oa.at[y, z // 2]
             oa[pl.ds(y, 1), pl.ds(z // 2, 1)] = own[None, None]
+            for t in (0, 1):
+
+                @pl.when(apart(z, t) > 2)
+                def _(t=t):
+                    straight(t, block, PH9A, lax.rem(y, 2))
+
             others(z, lambda t: send(block, block, LAST + apart(t, z) - 1, {"tp": t * 8 + y, "dp": one}, SENT_LAST))
-            forward_a(z)
+            across(block, SENT_ON[PH9A])
+            to_own_a(block)
             for distances in NEAREST:
                 (from_z if distances[0] % 2 == 0 else from_y)(distances)
 
@@ -603,8 +628,15 @@
         def _():
             block = ob.at[z, y // 2]
             ob[pl.ds(z, 1), pl.ds(y // 2, 1)] = own[None, None]
+            for t in (0, 1):
+
+                @pl.when(z != t)
+                def _(t=t):
+                    straight(t, block, PH9B, lax.rem(z, 2))
+
             others(y, lambda t: send(block, block, LAST + apart(t, y) - 1, {"tp": z * 8 + t, "dp": one}, SENT_LAST))
-            forward_b(y)
+            along(block, SENT_ON[PH9B])
+            to_own_b(block)
             for distances in NEAREST:
                 (from_y if distances[0] % 2 == 0 else from_z)(distances)
 
@@ -623,7 +655,20 @@
             assemble(1)
 
         with jax.named_scope("sent"):
-            wait_sent(w.at[0, pl.ds(0, 4), pl.ds(0, 7)], SENT_ON[PH9A])
+            wait_sent(r4.at[pl.ds(0, 7)], SENT_ON[PH9A])
+            for parity in range(2):
+                for low in range(2):
+
+                    @pl.when(jnp.logical_and(odd == parity, (z < 2) if low else (z > 1)))
+                    def _(parity=parity, low=low):
+                        wait_sent(oa.at[pl.ds(0, 5 + low), pl.ds(0, 4 - parity)], RELAY_B)
+                        wait_sent(oa.at[pl.ds(0, 7), pl.ds(0, 2 if low else 3 + parity)], RELAY_A)
+
+            for t in (0, 1):
+
+                @pl.when(jnp.where(odd == 0, apart(z, t) > 2, z != t))
+                def _(t=t):
+                    wait_sent(r4.at[pl.ds(0, 7)], LOW + t)
 
             @pl.when(lax.rem(y, 2) == 0)
             def _():

time: 54.3 us -> 53.3 us (0.982)
  Pallas kernels: 53.5 us -> 52.4 us
    pallas_call x1, Pallas kernels: 52.8 us -> 51.7 us  [body(): pl.pallas_call(kernel, name='decode', out_shape=(pltpu.VMEM((256, 512), B...]
where the time goes in v6:
time: 53.3 us; the launch traced here: 53 us
  Pallas kernels  52.4 us (98%)
  between operations  0.64 us (1%)
    pallas_call x1, Pallas kernels, body(): pl.pallas_call(kernel, name='decode', out_shape=(pltpu.VMEM((256, 512), B...  51.7 us

profile of v6, /device:TPU:1, one launch (start us, length us, event | category | flops | bytes accessed | tf_op | source)
XLA Modules:
  0.0 53.0 jit_solution(16102261234696931672)
XLA Ops:
  0.6 51.7 %decode.1 = (bf16[256,512]{1,0:T(8,128)(2,1)S(1)}, f32[2,2,32,128]{3,2,1,0:T(8,128)S(1)}) custom-call(bf16[256,512]{1,0:T(8,128)(2,1)} %tok_h.1, s32[1,32]{1,0:T(1,128)} %bitcast.5, f32[2,512]{1,0:T(2,128)} %gain_h.1, bf16[2,32,512]{2,1,0:T(8,128)(2,1)} %bitcast.3, f32[2,2]{1,0:T(2,128)} %ls_h.1, f32[2,2,64]{2,1,0:T(2,128)} %er_h.1, f32[2,2,64]{2,1,0:T(2,128)} %ei_h.1, ...), custom_call_target="tpu_custom_call" | custom-call | tf_op jit(solution)/shard_map/decode/pallas_call | solution.py:707
  52.3 0.7 %hand_over.1 = (bf16[256,512]{1,0:T(8,128)(2,1)}, f32[2,2,32,128]{3,2,1,0:T(8,128)}) custom-call(bf16[256,512]{1,0:T(8,128)(2,1)S(1)} %get-tuple-element.4.mixed, f32[2,2,32,128]{3,2,1,0:T(8,128)S(1)} %get-tuple-element.5.state), custom_call_target="tpu_custom_call" | custom-call | tf_op jit(solution)/shard_map/hand_over/pallas_call | solution.py:748

commit v7 on v6

--- a/solution.py
+++ b/solution.py
@@ -612,13 +612,14 @@
         def _():
             block = oa.at[y, z // 2]
             oa[pl.ds(y, 1), pl.ds(z // 2, 1)] = own[None, None]
-            for t in (0, 1):
-
+            def far_row(t):
                 @pl.when(apart(z, t) > 2)
-                def _(t=t):
+                def _():
                     straight(t, block, PH9A, lax.rem(y, 2))
 
+            far_row(0)
             others(z, lambda t: send(block, block, LAST + apart(t, z) - 1, {"tp": t * 8 + y, "dp": one}, SENT_LAST))
+            far_row(1)
             across(block, SENT_ON[PH9A])
             to_own_a(block)
             for distances in NEAREST:
@@ -628,13 +629,14 @@
         def _():
             block = ob.at[z, y // 2]
             ob[pl.ds(z, 1), pl.ds(y // 2, 1)] = own[None, None]
-            for t in (0, 1):
-
+            def other_row(t):
                 @pl.when(z != t)
-                def _(t=t):
+                def _():
                     straight(t, block, PH9B, lax.rem(z, 2))
 
+            other_row(0)
             others(y, lambda t: send(block, block, LAST + apart(t, y) - 1, {"tp": z * 8 + t, "dp": one}, SENT_LAST))
+            other_row(1)
             along(block, SENT_ON[PH9B])
             to_own_b(block)
             for distances in NEAREST:

time: 53.3 us -> 53.2 us (level)
  no operation moved by 1% of the time
where the time goes in v7:
time: 53.2 us; the launch traced here: 53 us
  Pallas kernels  52.4 us (98%)
  between operations  0.64 us (1%)
    pallas_call x1, Pallas kernels, body(): pl.pallas_call(kernel, name='decode', out_shape=(pltpu.VMEM((256, 512), B...  51.7 us

profile of v7, /device:TPU:1, one launch (start us, length us, event | category | flops | bytes accessed | tf_op | source)
XLA Modules:
  0.0 53.0 jit_solution(3896183662551281005)
XLA Ops:
  0.6 51.7 %decode.1 = (bf16[256,512]{1,0:T(8,128)(2,1)S(1)}, f32[2,2,32,128]{3,2,1,0:T(8,128)S(1)}) custom-call(bf16[256,512]{1,0:T(8,128)(2,1)} %tok_h.1, s32[1,32]{1,0:T(1,128)} %bitcast.5, f32[2,512]{1,0:T(2,128)} %gain_h.1, bf16[2,32,512]{2,1,0:T(8,128)(2,1)} %bitcast.3, f32[2,2]{1,0:T(2,128)} %ls_h.1, f32[2,2,64]{2,1,0:T(2,128)} %er_h.1, f32[2,2,64]{2,1,0:T(2,128)} %ei_h.1, ...), custom_call_target="tpu_custom_call" | custom-call | tf_op jit(solution)/shard_map/decode/pallas_call | solution.py:709
  52.3 0.7 %hand_over.1 = (bf16[256,512]{1,0:T(8,128)(2,1)}, f32[2,2,32,128]{3,2,1,0:T(8,128)}) custom-call(bf16[256,512]{1,0:T(8,128)(2,1)S(1)} %get-tuple-element.4.mixed, f32[2,2,32,128]{3,2,1,0:T(8,128)S(1)} %get-tuple-element.5.state), custom_call_target="tpu_custom_call" | custom-call | tf_op jit(solution)/shard_map/hand_over/pallas_call | solution.py:750

commit v8 on v7

--- a/solution.py
+++ b/solution.py
@@ -553,7 +553,7 @@
         core_a = 2 * x + lax.rem(y, 2)
         core_b = 2 * x + lax.rem(z, 2)
 
-        ORDER = (0, 1, 2, 7, 3, 6, 5, 4)
+        ORDER = (0, 2, 1, 7, 3, 6, 5, 4)
 
         def others(mine, serve, first=0):
             for t in ORDER:

time: 53.2 us -> 53.2 us (level)
  no operation moved by 1% of the time
where the time goes in v8:
time: 53.2 us; the launch traced here: 53 us
  Pallas kernels  52.4 us (98%)
  between operations  0.64 us (1%)
    pallas_call x1, Pallas kernels, body(): pl.pallas_call(kernel, name='decode', out_shape=(pltpu.VMEM((256, 512), B...  51.7 us

profile of v8, /device:TPU:1, one launch (start us, length us, event | category | flops | bytes accessed | tf_op | source)
XLA Modules:
  0.0 53.0 jit_solution(8523048040404700768)
XLA Ops:
  0.6 51.7 %decode.1 = (bf16[256,512]{1,0:T(8,128)(2,1)S(1)}, f32[2,2,32,128]{3,2,1,0:T(8,128)S(1)}) custom-call(bf16[256,512]{1,0:T(8,128)(2,1)} %tok_h.1, s32[1,32]{1,0:T(1,128)} %bitcast.5, f32[2,512]{1,0:T(2,128)} %gain_h.1, bf16[2,32,512]{2,1,0:T(8,128)(2,1)} %bitcast.3, f32[2,2]{1,0:T(2,128)} %ls_h.1, f32[2,2,64]{2,1,0:T(2,128)} %er_h.1, f32[2,2,64]{2,1,0:T(2,128)} %ei_h.1, ...), custom_call_target="tpu_custom_call" | custom-call | tf_op jit(solution)/shard_map/decode/pallas_call | solution.py:709
  52.3 0.7 %hand_over.1 = (bf16[256,512]{1,0:T(8,128)(2,1)}, f32[2,2,32,128]{3,2,1,0:T(8,128)}) custom-call(bf16[256,512]{1,0:T(8,128)(2,1)S(1)} %get-tuple-element.4.mixed, f32[2,2,32,128]{3,2,1,0:T(8,128)S(1)} %get-tuple-element.5.state), custom_call_target="tpu_custom_call" | custom-call | tf_op jit(solution)/shard_map/hand_over/pallas_call | solution.py:750
